TPU v7x, 32 devices: a whole 2x2x4 slice. The times are simulated.
32 devices in a mesh: ep: 8 (over z, x), tp: 4 (over y, core).
Axes of the slice: x: 2, y: 2, z: 4, core: 2. Of those that a mesh axis runs over, the one named last changes fastest.
Arguments:
- mixer_rows: bfloat16 [2048, 4096], P('ep'), may hold values from -8 to 8, as said below
- mixer_gain: float32 [4096], replicated, may hold values from 0.1 to 1.9
- gate_proj: bfloat16 [4096, 4096], P(None, 'tp'), may hold values from -0.09375 to 0.09375
- input_proj: bfloat16 [4096, 4096], P(None, 'tp'), may hold values from -0.09375 to 0.09375
- conv_taps: float32 [4, 4096], P(None, 'tp'), may hold values from -2 to 2
- input_gates: bfloat16 [16, 256, 256], P('tp'), may hold values from -0.375 to 0.375
- decay_gates: bfloat16 [16, 256, 256], P('tp'), may hold values from -0.375 to 0.375
- decay_offset: float32 [4096], P('tp'), may hold values from 4.8 to 13, as said below
- out_proj: bfloat16 [4096, 4096], P('tp'), may hold values from -0.09375 to 0.09375
- mixer_scale: float32 [4096], replicated, may hold values from 0.1 to 1.9
- expert_rows: bfloat16 [2048, 4096], P('ep'), may hold values from -6 to 6
- expert_gain: float32 [4096], replicated, may hold values from 0.1 to 1.9
- route_ids: int32 [2048, 2], P('ep'), may hold values from 0 to 7, all different within a row; in each aligned block of 256 rows (0 to 255, 256 to 511, ...) at most 96 rows name the same one
- route_weights: float32 [2048, 2], P('ep'), may hold values from 0.5 to 2
- expert_gate: bfloat16 [8, 4096, 1024], P('ep', None, 'tp'), may hold values from -0.09375 to 0.09375
- expert_up: bfloat16 [8, 4096, 1024], P('ep', None, 'tp'), may hold values from -0.09375 to 0.09375
- expert_down: bfloat16 [8, 1024, 4096], P('ep', 'tp'), may hold values from -0.1875 to 0.1875
- shared_gate: bfloat16 [4096, 1024], P(None, 'tp'), may hold values from -0.09375 to 0.09375
- shared_up: bfloat16 [4096, 1024], P(None, 'tp'), may hold values from -0.09375 to 0.09375
- shared_down: bfloat16 [1024, 4096], P('tp'), may hold values from -0.1875 to 0.1875
- expert_scale: float32 [4096], replicated, may hold values from 0.1 to 1.9
Outputs:
- mixer_out: bfloat16 [2048, 4096], P(('ep', 'tp'))
- expert_out: bfloat16 [2048, 4096], P(('ep', 'tp'))
Inputs may be any that keep to these rules, and one draw needn't show every extreme that they name: `mixer_rows`: order one, with a common direction whose weight drifts slowly along the sequence. `decay_offset`: the even channels forget within some 30 to 200 tokens; the odd channels keep 5 to 90 percent of their state over the whole sequence of 2048 tokens. `route_ids`: each row names 2 different experts; within the rows of one index of ep (aligned blocks of 256 rows) no expert is named by more than 96 rows, and in some blocks one is named by exactly 96.
All inputs are finite; a program needn't handle non-finite values.
Results may differ from a plain program's by a relative error of at most 0.0033.
The roundings to bfloat16 on the way count: a program that leaves them out, or rounds other values in their place, can miss the bound.
Values may be sent and summed in bfloat16 or wider, within the bound.
A program may use at most 192 MiB of HBM per device.

v0:
```python
import jax
import jax.numpy as jnp
from jax import lax
from jax.sharding import PartitionSpec as P

eps = 1e-06
lru_power = 8.0


def shifted(block, axis, distance):
    devices = range(lax.axis_size(axis))
    route = [(i - distance, i) for i in devices if i - distance in devices]
    return lax.ppermute(block, axis, route)


def prefix(value, axis, join, neutral):
    count, mine = (lax.axis_size(axis), lax.axis_index(axis))
    pieces = jax.tree.map(lambda part: lax.all_gather(part, axis), value)
    subtotal = jax.tree.map(
        lambda part, zero: jnp.full_like(part, 0) + jnp.asarray(zero, part.dtype), value, neutral
    )

    def step(position, subtotal):
        longer = join(subtotal, jax.tree.map(lambda part: part[position], pieces))
        return jax.tree.map(lambda new, old: jnp.where(position < mine, new, old), longer, subtotal)

    return lax.fori_loop(0, count - 1, step, subtotal)


def rms_scale(values, scale):
    floats = values.astype(jnp.float32)
    return floats * lax.rsqrt(jnp.mean(floats * floats, axis=-1, keepdims=True) + eps) * scale


def linear_pair(earlier, later):
    return (earlier[0] * later[0], later[0] * earlier[1] + later[1])


def slot_table(route_ids, expert_count, capacity):
    id_list = route_ids.reshape(-1)
    indicator = (id_list[:, None] == jnp.arange(expert_count, dtype=jnp.int32)[None, :]).astype(
        jnp.int32
    )
    earlier_count = jnp.cumsum(indicator, axis=0) - indicator
    position = jnp.sum(earlier_count * indicator, axis=1)
    slot_ids = id_list * capacity + position
    matched = (
        slot_ids[None, :] == jnp.arange(expert_count * capacity, dtype=jnp.int32)[:, None]
    ).astype(jnp.int32)
    source = jnp.sum(matched * jnp.arange(id_list.shape[0], dtype=jnp.int32)[None, :], axis=1)
    filled = jnp.sum(matched, axis=1) > 0
    return (slot_ids, source, filled)


def body(
    mixer_rows,
    mixer_gain,
    gate_proj,
    input_proj,
    conv_taps,
    input_gates,
    decay_gates,
    decay_offset,
    out_proj,
    mixer_scale,
    expert_rows,
    expert_gain,
    route_ids,
    route_weights,
    expert_gate,
    expert_up,
    expert_down,
    shared_gate,
    shared_up,
    shared_down,
    expert_scale,
):
    row_count = mixer_rows.shape[0]
    normed = rms_scale(mixer_rows, mixer_gain).astype(jnp.bfloat16)
    gate_branch = jax.nn.gelu(jnp.dot(normed, gate_proj, preferred_element_type=jnp.float32))
    branch = jnp.dot(normed, input_proj, preferred_element_type=jnp.float32).astype(jnp.bfloat16)
    tap_count = conv_taps.shape[0]
    earlier_rows = shifted(branch[row_count - tap_count + 1 :], "ep", 1)
    padded = jnp.concatenate([earlier_rows, branch], axis=0)
    conv_sum = conv_taps[0] * padded[0:row_count].astype(jnp.float32)
    for tap_index in range(1, tap_count):
        conv_sum = conv_sum + conv_taps[tap_index] * padded[
            tap_index : tap_index + row_count
        ].astype(jnp.float32)
    conv_out = conv_sum.astype(jnp.bfloat16)
    block_rows = conv_out.reshape(row_count, input_gates.shape[0], input_gates.shape[1])
    input_gate = jax.nn.sigmoid(
        jnp.einsum("rbi,bij->rbj", block_rows, input_gates, preferred_element_type=jnp.float32)
    ).reshape(row_count, -1)
    decay_gate = jax.nn.sigmoid(
        jnp.einsum("rbi,bij->rbj", block_rows, decay_gates, preferred_element_type=jnp.float32)
    ).reshape(row_count, -1)
    log_decay = -lru_power * decay_gate * jax.nn.softplus(-decay_offset)
    positions = lax.axis_index("ep") * row_count + jnp.arange(row_count, dtype=jnp.int32)
    input_scale = jnp.where((positions == 0)[:, None], 1.0, jnp.sqrt(-jnp.expm1(2.0 * log_decay)))
    drive_term = input_scale * input_gate * conv_out.astype(jnp.float32)
    decay_rate = jnp.exp(log_decay)
    decay_product, local_states = lax.associative_scan(
        linear_pair, (decay_rate, drive_term), axis=0
    )
    carried = prefix(
        (decay_product[-1], local_states[-1]),
        "ep",
        linear_pair,
        (jnp.ones_like(decay_rate[0]), jnp.zeros_like(decay_rate[0])),
    )
    states = local_states + decay_product * carried[1][None, :]
    gated_rows = (gate_branch * states).astype(jnp.bfloat16)
    mixer_term = jnp.dot(gated_rows, out_proj, preferred_element_type=jnp.float32)
    ep_size = lax.axis_size("ep")
    local_experts = expert_gate.shape[0]
    expert_count = local_experts * ep_size
    top_count = route_ids.shape[1]
    token_count = expert_rows.shape[0]
    row_width = expert_rows.shape[1]
    capacity = token_count * top_count * 3 // (2 * expert_count)
    expert_normed = rms_scale(expert_rows, expert_gain).astype(jnp.bfloat16)
    slot_ids, source, filled = slot_table(route_ids, expert_count, capacity)
    outgoing = jnp.where(
        filled[:, None], expert_normed[source // top_count], jnp.zeros((), jnp.bfloat16)
    )
    outgoing = outgoing.reshape(ep_size, local_experts, capacity, row_width)
    received = lax.all_to_all(outgoing, "ep", split_axis=0, concat_axis=0, tiled=True)
    gate_part = jnp.einsum(
        "secd,edf->secf", received, expert_gate, preferred_element_type=jnp.float32
    )
    up_part = jnp.einsum("secd,edf->secf", received, expert_up, preferred_element_type=jnp.float32)
    copy_hidden = (jax.nn.silu(gate_part) * up_part).astype(jnp.bfloat16)
    column_sums = lax.psum_scatter(
        jnp.einsum("secf,efd->secd", copy_hidden, expert_down, preferred_element_type=jnp.float32),
        "tp",
        scatter_dimension=3,
        tiled=True,
    )
    result = lax.all_to_all(column_sums, "ep", split_axis=0, concat_axis=0, tiled=True)
    flat_back = result.reshape(expert_count * capacity, -1)
    picked = flat_back[slot_ids] * route_weights.reshape(-1, 1)
    routed = jnp.sum(picked.reshape(token_count, top_count, -1), axis=1)
    shared_hidden = (
        jax.nn.silu(jnp.dot(expert_normed, shared_gate, preferred_element_type=jnp.float32))
        * jnp.dot(expert_normed, shared_up, preferred_element_type=jnp.float32)
    ).astype(jnp.bfloat16)
    shared_term = jnp.dot(shared_hidden, shared_down, preferred_element_type=jnp.float32)
    mixer_sum, expert_sum = (
        lax.psum_scatter(mixer_term, "tp", scatter_dimension=0, tiled=True),
        lax.psum_scatter(shared_term, "tp", scatter_dimension=0, tiled=True),
    )
    expert_sum = expert_sum + lax.all_to_all(routed, "tp", split_axis=0, concat_axis=1, tiled=True)
    mixer_out = rms_scale(mixer_sum, mixer_scale).astype(jnp.bfloat16)
    expert_out = rms_scale(expert_sum, expert_scale).astype(jnp.bfloat16)
    return (mixer_out, expert_out)


def solution(mesh):
    placed = (
        P("ep", None),
        P(),
        P(None, "tp"),
        P(None, "tp"),
        P(None, "tp"),
        P("tp", None, None),
        P("tp", None, None),
        P("tp"),
        P("tp", None),
        P(),
        P("ep", None),
        P(),
        P("ep", None),
        P("ep", None),
        P("ep", None, "tp"),
        P("ep", None, "tp"),
        P("ep", "tp", None),
        P(None, "tp"),
        P(None, "tp"),
        P("tp", None),
        P(),
    )
    return jax.shard_map(
        body,
        mesh=mesh,
        in_specs=placed,
        out_specs=(P(("ep", "tp"), None), P(("ep", "tp"), None)),
        check_vma=False,
    )
```

profile of v0, /device:TPU:1, one launch (start us, length us, event | category | flops | bytes accessed | tf_op | source)
XLA Modules:
  0.0 496.7 jit_solution(13850198637014624979)
XLA Ops:
  8.5 2.1 fusion.7
  12.7 3.6 fusion.9
  16.4 13.9 %gather_fusion = bf16[768,4096]{1,0:T(8,128)(2,1)} fusion(bf16[256,4096]{1,0:T(8,128)(2,1)} %fusion.9, s32[1024]{0:T(1024)S(1)} %pad_clamp_fusion.1), kind=kCustom, calls=%fused_computation | custom fusion | bytes 12585984 | tf_op jit(solution)/shard_map/gather | solution.py:125
  30.2 3.3 broadcast_select_fusion
  33.5 143.7 %all_to_all.29 = bf16[8,1,96,4096]{3,2,1,0:T(8,128)(2,1)S(1)} all-to-all(bf16[8,1,96,4096]{3,2,1,0:T(8,128)(2,1)S(1)} %broadcast_select_fusion), channel_id=1, replica_groups=mesh['ep'=8,'tp'=4] {'ep'}, dimensions={0} | all-to-all | bytes 12582912 | tf_op jit(solution)/shard_map/all_to_all | solution.py:128
  177.2 2.6 copy-done.3
  179.8 1.8 fusion.19
  181.6 14.5 %convolution_bitcast_fusion = f32[8,1,96,4096]{3,2,0,1:T(8,128)} fusion(bf16[1,256,4096]{2,1,0:T(8,128)(2,1)S(1)} %copy-done, bf16[1,4096,256]{2,1,0:T(8,128)(2,1)} %param.38, bf16[8,1,96,4096]{3,2,1,0:T(8,128)(2,1)} %copy-done.3, f32[8,1,96,256]{3,2,0,1:T(8,128)S(1)} %fusion.19), kind=kOutput, calls=%fused_computation.5 | convolution fusion | flops 3222405120 | bytes 23855104 | tf_op jit(solution)/shard_map/secf,efd->secd/dot_general | solution.py:135
  198.2 5.8 %convolution_convert_fusion = bf16[256,1024]{1,0:T(8,128)(2,1)S(1)} fusion(bf16[4096,1024]{1,0:T(8,128)(2,1)} %param.26, bf16[256,4096]{1,0:T(8,128)(2,1)S(1)} %copy-done.5, f32[4096]{0:T(1024)S(1)} %copy-done.32, f32[256]{0:T(256)S(1)} %add_rsqrt_fusion.1), kind=kOutput, calls=%fused_computation.39 | convolution fusion | flops 2151940096 | bytes 11027456 | tf_op jit(solution)/shard_map/dot_general | solution.py:81
  204.0 3.4 collective-permute-start
  208.5 1.9 fusion.15
  213.5 2.3 convert_multiply_fusion.4
  224.8 1.7 multiply_add_fusion
  229.6 2.0 multiply_add_fusion.1
  238.5 1.8 multiply_add_fusion.2
  294.6 2.8 pad.128
  297.4 2.7 pad.129
  300.3 2.8 pad.112
  303.0 2.7 pad.113
  306.5 24.2 %all-gather = f32[8,1,1024]{2,1,0:T(1,128)S(1)} all-gather(f32[1,1,1024]{2,1,0:T(1,128)S(1)} %add_bitcast_fusion.1), channel_id=1, replica_groups=mesh['ep'=8,'tp'=4] {'ep'}, dimensions={0}, use_global_device_ids=true | all-gather | bytes 36864 | tf_op jit(solution)/shard_map/all_gather | solution.py:18
  331.6 24.5 %all-gather.1 = f32[8,1,1024]{2,1,0:T(1,128)S(1)} all-gather(f32[1,1,1024]{2,1,0:T(1,128)S(1)} %add_bitcast_fusion), channel_id=1, replica_groups=mesh['ep'=8,'tp'=4] {'ep'}, dimensions={0}, use_global_device_ids=true | all-gather | bytes 36864 | tf_op jit(solution)/shard_map/all_gather | solution.py:18
  356.5 13.9 %fusion.68 = f32[256,4096]{1,0:T(8,128)} fusion(bf16[1024,4096]{1,0:T(8,128)(2,1)} %param.31, f32[256,1024]{1,0:T(8,128)} %pad.128, f32[256,1024]{1,0:T(8,128)} %pad.129, f32[256,1024]{1,0:T(8,128)} %pad.112, f32[256,1024]{1,0:T(8,128)} %pad.113, bf16[4096,1024]{1,0:T(8,128)(2,1)} %param.25, bf16[256,4096]{1,0:T(8,128)(2,1)S(1)} %copy-done.6, ...), kind=kOutput, calls=%fused_computation.68 | convolution fusion | flops 4302831616 | bytes 27284480 | tf_op jit(solution)/shard_map/dot_general | solution.py:114
  372.0 2.3 fusion.112
  374.3 6.5 %fusion.45 = f32[256,4096]{1,0:T(8,128)} fusion(bf16[256,4096]{1,0:T(8,128)(2,1)} %param.42, bf16[256,4096]{1,0:T(8,128)(2,1)S(1)} %copy-done.2, bf16[4096,256]{1,0:T(8,128)(2,1)} %param.41, f32[256,256]{1,0:T(8,128)S(1)} %fusion.112), kind=kOutput, calls=%fused_computation.45 | convolution fusion | flops 1074135040 | bytes 10747904 | tf_op jit(solution)/shard_map/dot_general | solution.py:148
  380.9 4.7 all-to-all-start.1
  386.1 43.5 %reduce-scatter.4.cloned.1.call-done = f32[64,4096]{1,0:T(8,128)} async-done(((f32[256,4096]{1,0:T(8,128)}), f32[64,4096]{1,0:T(8,128)}) %reduce-scatter.4.cloned.1.call-update) | async-done | bytes 1048592 | tf_op jit(solution)/shard_map/reduce_scatter | solution.py:150
  431.0 16.5 %all-to-all-done.1 = f32[8,1,96,1024]{3,2,1,0:T(8,128)} async-done(((f32[8,1,96,1024]{3,2,1,0:T(8,128)}), f32[8,1,96,1024]{3,2,1,0:T(8,128)}, u32[]{:S(2)}, u32[]{:S(2)}) %all-to-all-start.1) | async-done | bytes 3145760 | tf_op jit(solution)/shard_map/all_to_all | solution.py:140
  447.6 4.7 gather_fusion.1
  452.3 2.2 gather.13
  454.5 5.4 %multiply_reduce_fusion = f32[256,1024]{1,0:T(8,128)} fusion(f32[256,2,1024]{2,1,0:T(2,128)} %gather.13, f32[256,2]{1,0:T(8,128)S(1)} %copy.65), kind=kLoop, calls=%fused_computation.24 | loop fusion | flops 786432 | bytes 3147776 | tf_op jit(solution)/shard_map/reduce_sum | solution.py:143
  459.9 13.6 %all-to-all-start.2 = ((f32[4,64,1024]{2,1,0:T(8,128)}), f32[4,64,1024]{2,1,0:T(8,128)S(1)}, u32[]{:S(2)}, u32[]{:S(2)}) async-start(f32[4,64,1024]{2,1,0:T(8,128)} %bitcast.37), calls=%async_computation.5 | async-start | bytes 2097152 | tf_op jit(solution)/shard_map/all_to_all | solution.py:153
  474.5 12.5 %all-to-all-done.2 = f32[4,64,1024]{2,1,0:T(8,128)S(1)} async-done(((f32[4,64,1024]{2,1,0:T(8,128)}), f32[4,64,1024]{2,1,0:T(8,128)S(1)}, u32[]{:S(2)}, u32[]{:S(2)}) %all-to-all-start.2) | async-done | bytes 1048608 | tf_op jit(solution)/shard_map/all_to_all | solution.py:153
  (249 shorter events, 91.7 us)
Async XLA Ops:
  7.2 174.4 %copy-start = (bf16[1,256,4096]{2,1,0:T(8,128)(2,1)S(1)}, bf16[1,256,4096]{2,1,0:T(8,128)(2,1)}, u32[]{:S(2)}) copy-start(bf16[1,256,4096]{2,1,0:T(8,128)(2,1)} %param.39) | copy-start | bytes 6291460
  7.2 5.6 %copy-start.17 = (f32[4096]{0:T(1024)S(1)}, f32[4096]{0:T(1024)}, u32[]{:S(2)}) copy-start(f32[4096]{0:T(1024)} %param.34) | copy-start | bytes 49156
  7.2 373.7 %reduce-scatter.8.cloned.1.call-start = ((), (), s32[]{:S(2)}) async-start(), calls=%async_computation.8 | async-start | bytes 15728640 | tf_op jit(solution)/shard_map/reduce_scatter | solution.py:134
  33.5 146.2 %copy-start.30 = (bf16[1,4096,256]{2,1,0:T(8,128)(2,1)S(1)}, bf16[1,4096,256]{2,1,0:T(8,128)(2,1)}, u32[]{:S(2)}) copy-start(bf16[1,4096,256]{2,1,0:T(8,128)(2,1)} %param.37) | copy-start | bytes 6291460
  177.2 2.6 copy-start.3
  196.1 1.6 copy-start.5
  196.1 2.1 copy-start.32
  196.1 233.5 %reduce-scatter.4.cloned.1.call-start = ((), (), s32[]{:S(2)}) async-start(), calls=%async_computation.6 | async-start | bytes 5242880 | tf_op jit(solution)/shard_map/reduce_scatter | solution.py:150
  198.2 5.8 %copy-start.28 = (f32[256]{0:T(256)}, f32[256]{0:T(256)S(1)}, u32[]{:S(2)}) copy-start(f32[256]{0:T(256)S(1)} %add_rsqrt_fusion.1) | copy-start | bytes 3076
  198.2 9.2 %copy-start.26 = (f32[1024]{0:T(1024)S(1)}, f32[1024]{0:T(1024)}, u32[]{:S(2)}) copy-start(f32[1024]{0:T(1024)} %param.30) | copy-start | bytes 12292
  198.2 9.2 %copy-start.24 = (f32[4,1024]{1,0:T(4,128)S(1)}, f32[4,1024]{1,0:T(4,128)}, u32[]{:S(2)}) copy-start(f32[4,1024]{1,0:T(4,128)} %param.27) | copy-start | bytes 49156
  204.0 4.0 collective-permute-start
  208.5 2.3 copy-start.9
  279.0 11.5 %copy-start.15 = (f32[15,1024]{1,0:T(8,128)S(1)}, f32[15,1024]{1,0:T(8,128)}, u32[]{:S(2)}) copy-start(f32[15,1024]{1,0:T(8,128)} %slice.326) | copy-start | bytes 184324
  279.0 11.5 %copy-start.16 = (f32[15,1024]{1,0:T(8,128)S(1)}, f32[15,1024]{1,0:T(8,128)}, u32[]{:S(2)}) copy-start(f32[15,1024]{1,0:T(8,128)} %slice.293) | copy-start | bytes 184324
  283.9 6.5 %copy-start.23 = (f32[1,1024]{1,0:T(1,128)S(1)}, f32[1,1024]{1,0:T(1,128)}, u32[]{:S(2)}) copy-start(f32[1,1024]{1,0:T(1,128)} %slice.364) | copy-start | bytes 12292
  283.9 6.6 %copy-start.22 = (f32[1,1024]{1,0:T(1,128)S(1)}, f32[1,1024]{1,0:T(1,128)}, u32[]{:S(2)}) copy-start(f32[1,1024]{1,0:T(1,128)} %slice.390) | copy-start | bytes 12292
  285.7 4.9 copy-start.13
  285.8 4.9 copy-start.14
  294.6 5.6 %copy-start.10 = (f32[127,1024]{1,0:T(8,128)S(1)}, f32[127,1024]{1,0:T(8,128)}, u32[]{:S(2)}) copy-start(f32[127,1024]{1,0:T(8,128)} %get-tuple-element.133) | copy-start | bytes 1560580
  300.2 56.3 %copy-start.6 = (bf16[256,4096]{1,0:T(8,128)(2,1)S(1)}, bf16[256,4096]{1,0:T(8,128)(2,1)}, u32[]{:S(2)}) copy-start(bf16[256,4096]{1,0:T(8,128)(2,1)} %param.23) | copy-start | bytes 6291460
  300.2 56.3 %copy-start.29 = (f32[256]{0:T(256)S(1)}, f32[256]{0:T(256)}, u32[]{:S(2)}) copy-start(f32[256]{0:T(256)} %copy-done.28) | copy-start | bytes 3076
  300.2 56.3 %copy-start.33 = (f32[4096]{0:T(1024)S(1)}, f32[4096]{0:T(1024)}, u32[]{:S(2)}) copy-start(f32[4096]{0:T(1024)} %param.24) | copy-start | bytes 49156
  370.4 116.7 %reduce-scatter.6.cloned.1.call-start = ((), (), s32[]{:S(2)}) async-start(), calls=%async_computation.7 | async-start | bytes 5242880 | tf_op jit(solution)/shard_map/reduce_scatter | solution.py:151
  380.9 4.8 copy-start.25
  380.9 5.1 %copy-start.27 = (f32[256,2]{0,1:T(2,128)S(1)}, f32[256,2]{0,1:T(2,128)}, u32[]{:S(2)}) copy-start(f32[256,2]{0,1:T(2,128)} %param.36) | copy-start | bytes 6148
  380.9 66.6 %all-to-all-start.1 = ((f32[8,1,96,1024]{3,2,1,0:T(8,128)}), f32[8,1,96,1024]{3,2,1,0:T(8,128)}, u32[]{:S(2)}, u32[]{:S(2)}) async-start(f32[8,1,96,1024]{3,2,1,0:T(8,128)} %bitcast.135), calls=%async_computation.4 | async-start | bytes 6291456 | tf_op jit(solution)/shard_map/all_to_all | solution.py:140
  454.5 19.1 %copy-start.4 = (f32[64,4096]{1,0:T(8,128)S(1)}, f32[64,4096]{1,0:T(8,128)}, u32[]{:S(2)}) copy-start(f32[64,4096]{1,0:T(8,128)} %reduce-scatter.4.cloned.1.call-done) | copy-start | bytes 3145732
  454.5 19.1 %copy-start.18 = (f32[4096]{0:T(1024)S(1)}, f32[4096]{0:T(1024)}, u32[]{:S(2)}) copy-start(f32[4096]{0:T(1024)} %param.32) | copy-start | bytes 49156
  459.9 27.1 %all-to-all-start.2 = ((f32[4,64,1024]{2,1,0:T(8,128)}), f32[4,64,1024]{2,1,0:T(8,128)S(1)}, u32[]{:S(2)}, u32[]{:S(2)}) async-start(f32[4,64,1024]{2,1,0:T(8,128)} %bitcast.37), calls=%async_computation.5 | async-start | bytes 2097152 | tf_op jit(solution)/shard_map/all_to_all | solution.py:153
  487.1 1.7 copy-start.19
  487.1 2.6 copy-start.1
  (8 other events, 8.8 us)
Sparse Core Ops, SparseCore 0:
  196.2 97.2 reduce-scatter.7
  370.5 59.0 reduce-scatter.3
  432.1 44.5 reduce-scatter.5
where the time goes:
time: 506 us; the launch traced here: 497 us
  blocking collectives  192 us (38%)
  local copies, waits for them, and re-layouts  103 us (20%)
  waiting for transfers between devices  73.1 us (14%)
  matrix products  47.1 us (9%)
  other arithmetic  43.8 us (9%)
  starting transfers between devices  21.9 us (4%)
  between operations  15.2 us (3%)
    all_to_all x1, blocking collectives, body(): lax.all_to_all(outgoing, 'ep', split_axis=0, concat_axis=0, tiled=True)  144 us
    slice x52, local copies, waits for them, and re-layouts, body(): lax.associative_scan(linear_pair, (decay_rate, drive_term), axis=0)  58.3 us
    all_gather x2, blocking collectives, prefix(): pieces = jax.tree.map(lambda part: lax.all_gather(part, axis), value)  48.7 us
    reduce_scatter x1, waiting for transfers between devices, body(): lax.psum_scatter(mixer_term, 'tp', scatter_dimension=0, tiled=True)  43.5 us
    all_to_all x1, waiting for transfers between devices, body(): lax.all_to_all(column_sums, 'ep', split_axis=0, concat_axis=0, tiled=True)  16.5 us
    dot_general x1, matrix products, body(): jnp.einsum('secf,efd->secd', copy_hidden, expert_down, preferred_element_...  14.5 us
    dot_general x1, matrix products, body(): jnp.dot(gated_rows, out_proj, preferred_element_type=jnp.float32)  13.9 us
    gather x1, local copies, waits for them, and re-layouts, body(): expert_normed[source // top_count]  13.9 us
  transfers between devices with their start and end apart: 6, of which 4 were waited for; matrix products, arithmetic and copies ran while one was open for 28% of the time, Pallas kernels for 0%

commit v1 on v0

v1 whole, which is shorter than its diff:
```python
import functools

import jax
import jax.numpy as jnp
from jax import lax
from jax.experimental import pallas as pl
from jax.experimental.pallas import tpu as pltpu
from jax.sharding import PartitionSpec as P

eps = 1e-06
lru_power = 8.0
halo_rows = 16
MESH = pl.DeviceIdType.MESH
f32 = jnp.float32
bf16 = jnp.bfloat16


def rms_scale(values, scale):
    floats = values.astype(f32)
    return floats * lax.rsqrt(jnp.mean(floats * floats, axis=-1, keepdims=True) + eps) * scale


def remote(src, dst, send_sem, recv_sem, ep_at, tp_at):
    return pltpu.make_async_remote_copy(
        src_ref=src,
        dst_ref=dst,
        send_sem=send_sem,
        recv_sem=recv_sem,
        device_id=(ep_at, tp_at),
        device_id_type=MESH,
    )


def greet(peers):
    barrier = pltpu.get_barrier_semaphore()
    for ep_at, tp_at in peers:
        pl.semaphore_signal(barrier, inc=1, device_id=(ep_at, tp_at), device_id_type=MESH)
    pl.semaphore_wait(barrier, len(peers))


def expm1_neg(y):
    series = y * (1 + y / 2 * (1 + y / 3 * (1 + y / 4 * (1 + y / 5 * (1 + y / 6 * (1 + y / 7))))))
    return jnp.where(y > -0.35, series, jnp.exp(y) - 1.0)


def mixer_kernel(
    ep, branch_ref, gate_ref, taps_ref, ig_ref, dg_ref, soft_ref, out_ref,
    ext, halo, a_buf, b_buf, ends, got, halo_send, halo_recv, end_send, end_recv,
):
    me, t = lax.axis_index("ep"), lax.axis_index("tp")
    rows, width = branch_ref.shape
    blocks, bw = ig_ref.shape[0], ig_ref.shape[1]
    greet([(lax.rem(me + i, ep), t) for i in range(1, ep)])
    nxt = remote(
        branch_ref.at[pl.ds(rows - halo_rows, halo_rows)], halo,
        halo_send, halo_recv, lax.rem(me + 1, ep), t,
    )
    nxt.start()
    ext[pl.ds(halo_rows, rows), :] = branch_ref[...].astype(f32)
    nxt.wait()
    ext[pl.ds(0, halo_rows), :] = jnp.where(me == 0, 0.0, halo[...].astype(f32))
    taps = taps_ref.shape[0]
    base = halo_rows - (taps - 1)
    first = (lax.broadcasted_iota(jnp.int32, (rows, bw), 0) == 0) & (me == 0)
    for b in range(blocks):
        cols = pl.ds(b * bw, bw)
        acc = taps_ref[0:1, cols] * ext[pl.ds(base, rows), cols]
        for k in range(1, taps):
            acc = acc + taps_ref[k : k + 1, cols] * ext[pl.ds(base + k, rows), cols]
        conv = acc.astype(bf16)
        ig = jax.nn.sigmoid(jnp.dot(conv, ig_ref[b], preferred_element_type=f32))
        dg = jax.nn.sigmoid(jnp.dot(conv, dg_ref[b], preferred_element_type=f32))
        ld = -lru_power * dg * soft_ref[0:1, cols]
        scale = jnp.where(first, 1.0, jnp.sqrt(-expm1_neg(2.0 * ld)))
        a_buf[:, cols] = jnp.exp(ld)
        b_buf[:, cols] = scale * ig * conv.astype(f32)

    row = lax.broadcasted_iota(jnp.int32, (8, width), 0)

    def block(r, carry):
        pc, sc = carry
        at = pl.ds(pl.multiple_of(r * 8, 8), 8)
        a, b = a_buf[at, :], b_buf[at, :]
        for sh in (1, 2, 4):
            keep = row >= sh
            b = jnp.where(keep, b + a * pltpu.roll(b, sh, 0), b)
            a = jnp.where(keep, a * pltpu.roll(a, sh, 0), a)
        b = b + a * sc
        a = a * pc
        a_buf[at, :] = a
        b_buf[at, :] = b
        return a[7:8, :], b[7:8, :]

    pl_last, s_last = lax.fori_loop(
        0, rows // 8, block, (jnp.ones((1, width), f32), jnp.zeros((1, width), f32))
    )
    ends[...] = jnp.where(row == 0, pl_last, s_last)
    copies = [
        remote(ends, got.at[i], end_send.at[i], end_recv.at[i], lax.rem(me + i, ep), t)
        for i in range(1, ep)
    ]
    for c in copies:
        c.start()
    for c in copies:
        c.wait()
    carry = jnp.zeros((1, width), f32)
    for i in range(ep - 1, 0, -1):
        carry = jnp.where(me >= i, got[i, 0:1, :] * carry + got[i, 1:2, :], carry)

    def finish(r, _):
        at = pl.ds(pl.multiple_of(r * 16, 16), 16)
        out_ref[at, :] = (gate_ref[at, :] * (b_buf[at, :] + a_buf[at, :] * carry)).astype(bf16)
        return 0

    lax.fori_loop(0, rows // 16, finish, 0)


def moe_kernel(
    ep, tp, outq, eg_hbm, eu_hbm, ed, back,
    recv, eg, eu, wd, hid, ret, load_sem,
    z_s, z_r, y_s, y_r, c_s, c_r, hy_s, hy_r, hc_s, hc_r, w_s, w_r, b_s, b_r,
):
    me, t = lax.axis_index("ep"), lax.axis_index("tp")
    ys = tp // 2
    y, c = t // 2, lax.rem(t, 2)
    mate = y * 2 + 1 - c
    dq = outq.shape[2]

    def up(k):
        return lax.rem(y + k, ys) * 2 + c

    def down_of(k, core):
        return lax.rem(y + ys - k, ys) * 2 + core

    greet(
        [(lax.rem(me + i, ep), t) for i in range(1, ep)]
        + [(me, lax.rem(t + i, tp)) for i in range(1, tp)]
    )

    def z_copy(i):
        return remote(
            outq.at[i], recv.at[t, i], z_s.at[i], z_r.at[i], lax.rem(me + i, ep), t
        )

    def y_copy(k, i):
        return remote(recv.at[t, i], recv.at[t, i], y_s.at[k, i], y_r.at[k, i], me, up(k))

    def c_copy(k, i):
        q = down_of(k, c)
        return remote(recv.at[q, i], recv.at[q, i], c_s.at[k, i], c_r.at[k, i], me, mate)

    def hy_copy(k, i):
        return remote(hid.at[t, i], hid.at[t, i], hy_s.at[k, i], hy_r.at[k, i], me, up(k))

    def hc_copy(k, i):
        q = down_of(k, c)
        return remote(hid.at[q, i], hid.at[q, i], hc_s.at[k, i], hc_r.at[k, i], me, mate)

    def w_copy(i):
        q = lax.rem(t + i, tp)
        return remote(
            ed.at[:, pl.ds(pl.multiple_of(q * dq, dq), dq)], wd.at[t],
            w_s.at[i], w_r.at[i], me, q,
        )

    def b_copy(i):
        return remote(
            ret.at[i], back.at[i], b_s.at[i], b_r.at[i], lax.rem(me + ep - i, ep), t
        )

    for i in range(1, ep):
        z_copy(i).start()
    loads = [
        pltpu.make_async_copy(outq.at[0], recv.at[t, 0], load_sem.at[0]),
        pltpu.make_async_copy(eg_hbm, eg, load_sem.at[1]),
        pltpu.make_async_copy(eu_hbm, eu, load_sem.at[2]),
        pltpu.make_async_copy(
            ed.at[:, pl.ds(pl.multiple_of(t * dq, dq), dq)], wd.at[t], load_sem.at[3]
        ),
    ]
    for load in loads:
        load.start()
    for load in loads:
        load.wait()

    def step(n, _):
        @pl.when(n < ep)
        def _():
            i = n

            @pl.when(i > 0)
            def _():
                z_copy(i).wait_recv()

            for k in range(1, ys):
                y_copy(k, i).start()
            c_copy(0, i).start()

        @pl.when(n == 1)
        def _():
            for i in range(1, tp):
                w_copy(i).start()

        @pl.when((n >= 1) & (n < ep + 1))
        def _():
            i = n - 1
            for k in range(1, ys):
                y_copy(k, i).wait_recv()
                c_copy(k, i).start()

        @pl.when((n >= 2) & (n < ep + 2))
        def _():
            i = n - 2
            for k in range(ys):
                c_copy(k, i).wait_recv()
            gate = up_sum = None
            for q in range(tp):
                x = recv[q, i]
                span = pl.ds(q * dq, dq)
                g = jnp.dot(x, eg[span, :], preferred_element_type=f32)
                u = jnp.dot(x, eu[span, :], preferred_element_type=f32)
                gate = g if gate is None else gate + g
                up_sum = u if up_sum is None else up_sum + u
            hid[t, i] = (jax.nn.silu(gate) * up_sum).astype(bf16)
            for k in range(1, ys):
                hy_copy(k, i).start()
            hc_copy(0, i).start()

        @pl.when((n >= 3) & (n < ep + 3))
        def _():
            i = n - 3
            for k in range(1, ys):
                hy_copy(k, i).wait_recv()
                hc_copy(k, i).start()

        @pl.when(n == 4)
        def _():
            for i in range(1, tp):
                w_copy(i).wait()

        @pl.when(n >= 4)
        def _():
            i = n - 4
            for k in range(ys):
                hc_copy(k, i).wait_recv()
            total = jnp.dot(hid[0, i], wd[0], preferred_element_type=f32)
            for q in range(1, tp):
                total = total + jnp.dot(hid[q, i], wd[q], preferred_element_type=f32)

            @pl.when(i == 0)
            def _():
                back[0] = total.astype(bf16)

            @pl.when(i > 0)
            def _():
                ret[i] = total.astype(bf16)
                b_copy(i).start()

        return 0

    lax.fori_loop(0, ep + 4, step, 0)

    def settle(i, _):
        for k in range(1, ys):
            y_copy(k, i).wait_send()
            hy_copy(k, i).wait_send()
        for k in range(ys):
            c_copy(k, i).wait_send()
            hc_copy(k, i).wait_send()

        @pl.when(i > 0)
        def _():
            z_copy(i).wait_send()
            b_copy(i).wait()

        return 0

    lax.fori_loop(0, ep, settle, 0)


def final_kernel(
    tp, m_ref, e_ref, ms_ref, es_ref, mo_ref, eo_ref,
    m_half, e_half, m_out, m_in, e_in, md_s, md_r, ed_s, ed_r, my_s, my_r, ey_s, ey_r,
):
    me, t = lax.axis_index("ep"), lax.axis_index("tp")
    ys = tp // 2
    y, c = t // 2, lax.rem(t, 2)
    mate = y * 2 + 1 - c

    def at_y(k):
        return lax.rem(y + k, ys)

    greet([(me, mate)] + [(me, at_y(k) * 2 + c) for k in range(1, ys)])
    order = list(range(1, ys)) + [0]

    def pair(ref, half, s, r, k):
        q = at_y(k) * 2 + 1 - c
        return remote(ref.at[q], half.at[k], s.at[k], r.at[k], me, mate)

    for k in order:
        pair(m_ref, m_half, md_s, md_r, k).start()
    for k in order:
        pair(e_ref, e_half, ed_s, ed_r, k).start()

    def my_copy(k):
        return remote(m_out.at[k], m_in.at[k], my_s.at[k], my_r.at[k], me, at_y(k) * 2 + c)

    def ey_copy(k):
        return remote(e_half.at[k], e_in.at[k], ey_s.at[k], ey_r.at[k], me, at_y(k) * 2 + c)

    for k in range(1, ys):
        pair(m_ref, m_half, md_s, md_r, k).wait_recv()
        m_out[k] = (m_half[k] + m_ref[at_y(k) * 2 + c]).astype(bf16)
        my_copy(k).start()
    for k in range(1, ys):
        pair(e_ref, e_half, ed_s, ed_r, k).wait_recv()
        e_half[k] = e_half[k] + e_ref[at_y(k) * 2 + c]
        ey_copy(k).start()
    pair(m_ref, m_half, md_s, md_r, 0).wait_recv()
    total = m_half[0] + m_ref[t]
    for k in range(1, ys):
        my_copy(k).wait_recv()
        total = total + m_in[k].astype(f32)
    mo_ref[...] = rms_scale(total, ms_ref[...]).astype(bf16)
    pair(e_ref, e_half, ed_s, ed_r, 0).wait_recv()
    total = e_half[0] + e_ref[t]
    for k in range(1, ys):
        ey_copy(k).wait_recv()
        total = total + e_in[k]
    eo_ref[...] = rms_scale(total, es_ref[...]).astype(bf16)
    for k in range(ys):
        pair(m_ref, m_half, md_s, md_r, k).wait_send()
        pair(e_ref, e_half, ed_s, ed_r, k).wait_send()
    for k in range(1, ys):
        my_copy(k).wait_send()
        ey_copy(k).wait_send()


def vmem(n):
    return [pl.BlockSpec(memory_space=pltpu.VMEM)] * n


def dma(*shape):
    return pltpu.SemaphoreType.DMA(shape)


def params(number):
    return pltpu.CompilerParams(
        collective_id=number, has_side_effects=True, vmem_limit_bytes=60 * 1024 * 1024
    )


def recurrence(ep, branch, gate_branch, conv_taps, input_gates, decay_gates, soft):
    rows, width = branch.shape
    return pl.pallas_call(
        functools.partial(mixer_kernel, ep),
        out_shape=jax.ShapeDtypeStruct((rows, width), bf16),
        in_specs=vmem(6),
        out_specs=vmem(1)[0],
        scratch_shapes=[
            pltpu.VMEM((halo_rows + rows, width), f32),
            pltpu.VMEM((halo_rows, width), bf16),
            pltpu.VMEM((rows, width), f32),
            pltpu.VMEM((rows, width), f32),
            pltpu.VMEM((8, width), f32),
            pltpu.VMEM((ep, 8, width), f32),
            pltpu.SemaphoreType.DMA,
            pltpu.SemaphoreType.DMA,
            dma(ep),
            dma(ep),
        ],
        compiler_params=params(0),
        name="recurrence",
    )(branch, gate_branch, conv_taps, input_gates, decay_gates, soft)


def experts(ep, tp, outq, expert_gate, expert_up, expert_down):
    _, cap, dq = outq.shape
    depth, hf = expert_gate.shape
    ys = tp // 2
    return pl.pallas_call(
        functools.partial(moe_kernel, ep, tp),
        out_shape=jax.ShapeDtypeStruct((ep, cap, dq), bf16),
        in_specs=vmem(1) + [pl.BlockSpec(memory_space=pl.ANY)] * 3,
        out_specs=vmem(1)[0],
        scratch_shapes=[
            pltpu.VMEM((tp, ep, cap, dq), bf16),
            pltpu.VMEM((depth, hf), bf16),
            pltpu.VMEM((depth, hf), bf16),
            pltpu.VMEM((tp, hf, dq), bf16),
            pltpu.VMEM((tp, ep, cap, hf), bf16),
            pltpu.VMEM((ep, cap, dq), bf16),
            dma(4),
            dma(ep), dma(ep),
            dma(ys, ep), dma(ys, ep),
            dma(ys, ep), dma(ys, ep),
            dma(ys, ep), dma(ys, ep),
            dma(ys, ep), dma(ys, ep),
            dma(tp), dma(tp),
            dma(ep), dma(ep),
        ],
        compiler_params=params(1),
        name="experts",
    )(outq, expert_gate, expert_up, expert_down)


def final(tp, mixer_term, expert_term, mixer_scale, expert_scale):
    rows, width = mixer_term.shape
    each, ys = rows // tp, tp // 2
    return pl.pallas_call(
        functools.partial(final_kernel, tp),
        out_shape=[jax.ShapeDtypeStruct((each, width), bf16)] * 2,
        in_specs=vmem(4),
        out_specs=vmem(2),
        scratch_shapes=[
            pltpu.VMEM((ys, each, width), f32),
            pltpu.VMEM((ys, each, width), f32),
            pltpu.VMEM((ys, each, width), bf16),
            pltpu.VMEM((ys, each, width), bf16),
            pltpu.VMEM((ys, each, width), f32),
            dma(ys), dma(ys), dma(ys), dma(ys),
            dma(ys), dma(ys), dma(ys), dma(ys),
        ],
        compiler_params=params(2),
        name="final",
    )(
        mixer_term.reshape(tp, each, width),
        expert_term.reshape(tp, each, width),
        mixer_scale.reshape(1, -1),
        expert_scale.reshape(1, -1),
    )


def body(
    mixer_rows, mixer_gain, gate_proj, input_proj, conv_taps, input_gates, decay_gates,
    decay_offset, out_proj, mixer_scale, expert_rows, expert_gain, route_ids, route_weights,
    expert_gate, expert_up, expert_down, shared_gate, shared_up, shared_down, expert_scale,
):
    ep, tp = lax.axis_size("ep"), lax.axis_size("tp")
    me, t = lax.axis_index("ep"), lax.axis_index("tp")
    tokens, width = expert_rows.shape
    top = route_ids.shape[1]
    cap = tokens * top * 3 // (2 * ep)
    dq = width // tp

    expert_normed = rms_scale(expert_rows, expert_gain).astype(bf16)
    offset_ids = lax.rem(route_ids + (ep - me), ep)
    indicator = jnp.sum(
        (offset_ids[:, :, None] == jnp.arange(ep, dtype=jnp.int32)).astype(f32), axis=1
    )
    below = (
        jnp.arange(tokens)[:, None] > jnp.arange(tokens)[None, :]
    ).astype(bf16)
    earlier = jnp.dot(below, indicator.astype(bf16), preferred_element_type=f32)
    chosen = (offset_ids[:, :, None] == jnp.arange(ep, dtype=jnp.int32)).astype(f32)
    position = jnp.sum(chosen * earlier[:, None, :], axis=2).astype(jnp.int32)
    slot_ids = offset_ids * cap + position
    slots = jnp.arange(ep * cap, dtype=jnp.int32)
    picks = [(slot_ids[:, k][:, None] == slots[None, :]).astype(bf16) for k in range(top)]
    placed = sum(picks[1:], picks[0])
    quarter = lax.dynamic_slice_in_dim(expert_normed, t * dq, dq, axis=1)
    outq = lax.dot_general(
        placed, quarter, (((0,), (0,)), ((), ())), preferred_element_type=f32
    ).astype(bf16).reshape(ep, cap, dq)
    back = experts(ep, tp, outq, expert_gate[0], expert_up[0], expert_down[0])

    normed = rms_scale(mixer_rows, mixer_gain).astype(bf16)
    gate_branch = jax.nn.gelu(jnp.dot(normed, gate_proj, preferred_element_type=f32))
    branch = jnp.dot(normed, input_proj, preferred_element_type=f32).astype(bf16)
    soft = jax.nn.softplus(-decay_offset).reshape(1, -1)
    gated = recurrence(ep, branch, gate_branch, conv_taps, input_gates, decay_gates, soft)
    mixer_term = jnp.dot(gated, out_proj, preferred_element_type=f32)

    shared_hidden = (
        jax.nn.silu(jnp.dot(expert_normed, shared_gate, preferred_element_type=f32))
        * jnp.dot(expert_normed, shared_up, preferred_element_type=f32)
    ).astype(bf16)
    shared_term = jnp.dot(shared_hidden, shared_down, preferred_element_type=f32)
    flat = back.reshape(ep * cap, dq)
    routed = sum(
        route_weights[:, k : k + 1] * jnp.dot(picks[k], flat, preferred_element_type=f32)
        for k in range(top)
    )
    mine = lax.dynamic_slice_in_dim(shared_term, t * dq, dq, axis=1)
    expert_term = lax.dynamic_update_slice_in_dim(shared_term, mine + routed, t * dq, axis=1)
    return tuple(final(tp, mixer_term, expert_term, mixer_scale, expert_scale))


def solution(mesh):
    placed = (
        P("ep", None),
        P(),
        P(None, "tp"),
        P(None, "tp"),
        P(None, "tp"),
        P("tp", None, None),
        P("tp", None, None),
        P("tp"),
        P("tp", None),
        P(),
        P("ep", None),
        P(),
        P("ep", None),
        P("ep", None),
        P("ep", None, "tp"),
        P("ep", None, "tp"),
        P("ep", "tp", None),
        P(None, "tp"),
        P(None, "tp"),
        P("tp", None),
        P(),
    )
    return jax.shard_map(
        body,
        mesh=mesh,
        in_specs=placed,
        out_specs=(P(("ep", "tp"), None), P(("ep", "tp"), None)),
        check_vma=False,
    )
```

time: 506 us -> 211 us (0.42); the launches traced: 497 us -> 210 us
  blocking collectives: 192 us -> 0 us
  Pallas kernels: 0 us -> 164 us
  local copies, waits for them, and re-layouts: 103 us -> 5.32 us
  waiting for transfers between devices: 73.1 us -> 0 us
  other arithmetic: 43.8 us -> 5.58 us
  starting transfers between devices: 21.9 us -> 0 us
  between operations: 15.2 us -> 0.79 us
  matrix products: 47.1 us -> 35 us
    pallas_call x0 -> x3, Pallas kernels: none -> 164 us  [the longest x1 102 us: experts(): pl.pallas_call(functools.partial(moe_kernel, ep, tp), out_shape=jax.Shape...]
    all_to_all x1 -> x0, blocking collectives: 144 us -> none  [body(): lax.all_to_all(outgoing, 'ep', split_axis=0, concat_axis=0, tiled=True)]
    slice x55 -> x2, local copies, waits for them, and re-layouts: 58.5 us -> 0.01 us  [the longest x1 0.01 us: body(): slot_ids[:, k][:, None] == slots[None, :]]
    all_gather x2 -> x0, blocking collectives: 48.7 us -> none  [prefix(): pieces = jax.tree.map(lambda part: lax.all_gather(part, axis), value)]
    reduce_scatter x3 -> x0, waiting for transfers between devices: 43.5 us -> none  [the longest x1 43.5 us: body(): lax.psum_scatter(mixer_term, 'tp', scatter_dimension=0, tiled=True)]
    all_to_all x2 -> x0, waiting for transfers between devices: 29 us -> none  [the longest x1 16.5 us: body(): lax.all_to_all(column_sums, 'ep', split_axis=0, concat_axis=0, tiled=True)]
    gather x3 -> x0, local copies, waits for them, and re-layouts: 20.8 us -> none  [the longest x1 13.9 us: body(): expert_normed[source // top_count]]
    all_to_all x2 -> x0, starting transfers between devices: 18.4 us -> none  [the longest x1 13.6 us: body(): lax.all_to_all(routed, 'tp', split_axis=0, concat_axis=1, tiled=True)]
  transfers between devices with their start and end apart: 6 -> 0, of which waited for: 4 -> 0; matrix products, arithmetic and copies ran while one was open for 28% -> 0% of each run, Pallas kernels for 0% -> 0%
where the time goes in v1:
time: 211 us; the launch traced here: 210 us
  Pallas kernels  164 us (78%)
  matrix products  35 us (17%)
  other arithmetic  5.58 us (3%)
  local copies, waits for them, and re-layouts  5.32 us (3%)
    pallas_call x1, Pallas kernels, experts(): pl.pallas_call(functools.partial(moe_kernel, ep, tp), out_shape=jax.Shape...  102 us
    pallas_call x1, Pallas kernels, final(): pl.pallas_call(functools.partial(final_kernel, tp), out_shape=[jax.ShapeD...  45.3 us
    pallas_call x1, Pallas kernels, recurrence(): pl.pallas_call(functools.partial(mixer_kernel, ep), out_shape=jax.ShapeDt...  16.5 us
    dot_general x1, matrix products, body(): mixer_term = jnp.dot(gated, out_proj, preferred_element_type=f32)  7.84 us
    dot_general x1, matrix products, body(): jnp.dot(normed, gate_proj, preferred_element_type=f32)  7.28 us
    dot_general x1, matrix products, body(): jnp.dot(shared_hidden, shared_down, preferred_element_type=f32)  6.56 us
    dot_general x2, matrix products, body(): jnp.dot(picks[k], flat, preferred_element_type=f32)  5.67 us
    unnamed x24, local copies, waits for them, and re-layouts  5.31 us

profile of v1, /device:TPU:1, one launch (start us, length us, event | category | flops | bytes accessed | tf_op | source)
XLA Modules:
  0.0 210.3 jit_solution(10725268744575771992)
XLA Ops:
  0.6 0.0 copy-start
  0.6 0.0 copy-start.5
  0.7 0.8 compare_select_fusion.1
  1.5 0.2 fusion.38
  1.7 0.7 convert_add_fusion
  2.4 0.0 copy-start.3
  2.4 2.2 %fusion.3 = f32[256]{0:T(256)S(1)} fusion(bf16[256,4096]{1,0:T(8,128)(2,1)} %param.31), kind=kLoop, calls=%fused_computation.7 | loop fusion | flops 3145472 | bytes 2098176 | tf_op jit(solution)/shard_map/reduce_sum | solution.py:20
  4.7 0.0 copy-done.5
  4.7 0.0 copy-done.3
  4.7 0.6 fusion.5
  5.3 0.0 copy-start.1
  5.3 1.3 copy-done.1
  6.7 1.9 convolution_convert_fusion
  8.6 101.7 %experts.1 = bf16[8,96,1024]{2,1,0:T(8,128)(2,1)} custom-call(bf16[8,96,1024]{2,1,0:T(8,128)(2,1)} %bitcast.33, bf16[4096,256]{1,0:T(8,128)(2,1)} %bitcast.30, bf16[4096,256]{1,0:T(8,128)(2,1)} %bitcast.31, bf16[256,4096]{1,0:T(8,128)(2,1)} %bitcast.32), custom_call_target="tpu_custom_call" | custom-call | tf_op jit(solution)/shard_map/experts/pallas_call | solution.py:381
  110.3 0.0 copy-start.2
  110.3 0.0 copy-done.7
  110.3 2.2 %convolution_multiply_fusion.1 = f32[256,1024]{1,0:T(8,128)S(1)} fusion(bf16[768,1024]{1,0:T(8,128)(2,1)} %bitcast.27, f32[256]{0:T(256)S(1)} %bitcast.42, s32[256]{0:T(256)S(1)} %bitcast.40), kind=kOutput, calls=%fused_computation.16 | convolution fusion | flops 403111936 | bytes 2623488 | tf_op jit(solution)/shard_map/dot_general | solution.py:481
  112.5 0.0 copy-done.2
  112.5 2.3 %fusion.47 = f32[256,256]{1,0:T(8,128)S(1)} fusion(bf16[256,4096]{1,0:T(8,128)(2,1)S(1)} %copy-done.2, bf16[4096,256]{1,0:T(8,128)(2,1)} %param.38), kind=kOutput, calls=%fused_computation.63 | convolution fusion | flops 536870912 | bytes 4456448 | tf_op jit(solution)/shard_map/dot_general | solution.py:475
  114.8 6.6 %fusion.10 = f32[256,4096]{1,0:T(8,128)} fusion(bf16[256,4096]{1,0:T(8,128)(2,1)S(1)} %copy-done, bf16[256,4096]{1,0:T(8,128)(2,1)} %copy-done.1, bf16[4096,256]{1,0:T(8,128)(2,1)} %param.39, f32[256,256]{1,0:T(8,128)S(1)} %fusion.47), kind=kOutput, calls=%fused_computation.20 | convolution fusion | flops 1074135040 | bytes 10747904 | tf_op jit(solution)/shard_map/dot_general | solution.py:478
  121.4 3.5 %fusion.8 = f32[256,4096]{1,0:T(8,128)} fusion(f32[256,4096]{1,0:T(8,128)} %fusion.10, s32[]{:T(128)S(6)} %select_n.10, f32[256,1024]{1,0:T(8,128)S(1)} %convolution_multiply_fusion.1, bf16[768,1024]{1,0:T(8,128)(2,1)} %bitcast.28, f32[256]{0:T(256)S(1)} %bitcast.41, s32[256]{0:T(256)S(1)} %bitcast.38), kind=kOutput, calls=%fused_computation.15 | convolution fusion | flops 403636224 | bytes 4720644 | tf_op jit(solution)/shard_map/dot_general | solution.py:481
  124.9 0.5 fusion
  125.4 0.2 copy-done.8
  125.6 7.3 %fusion.17.gate_ref = f32[256,1024]{1,0:T(8,128)} fusion(bf16[4096,1024]{1,0:T(8,128)(2,1)} %param.23, bf16[256,4096]{1,0:T(8,128)(2,1)S(1)} %copy-done.4, f32[4096]{0:T(1024)S(1)} %copy-done.8, f32[256]{0:T(256)S(1)} %add_rsqrt_fusion.1), kind=kOutput, calls=%fused_computation.27 | convolution fusion | flops 2153775104 | bytes 11551744 | tf_op jit(solution)/shard_map/dot_general | solution.py:468
  132.9 0.0 slice-done.1
  132.9 3.3 %convolution_convert_fusion.1.branch_ref = bf16[256,1024]{1,0:T(8,128)(2,1)} fusion(bf16[4096,1024]{1,0:T(8,128)(2,1)S(1)} %bitcast.44, bf16[256,4096]{1,0:T(8,128)(2,1)S(1)} %copy-done.4, f32[4096]{0:T(1024)S(1)} %copy-done.8, f32[256]{0:T(256)S(1)} %add_rsqrt_fusion.1), kind=kOutput, calls=%fused_computation.17 | convolution fusion | flops 2151940096 | bytes 11027456 | tf_op jit(solution)/shard_map/dot_general | solution.py:469
  136.2 0.6 compare_select_fusion
  136.8 16.5 %recurrence.1 = bf16[256,1024]{1,0:T(8,128)(2,1)} custom-call(bf16[256,1024]{1,0:T(8,128)(2,1)} %convolution_convert_fusion.1.branch_ref, f32[256,1024]{1,0:T(8,128)} %fusion.17.gate_ref, f32[4,1024]{1,0:T(4,128)} %taps_ref.1, bf16[4,256,256]{2,1,0:T(8,128)(2,1)} %ig_ref.1, bf16[4,256,256]{2,1,0:T(8,128)(2,1)} %dg_ref.1, f32[1,1024]{1,0:T(1,128)} %bitcast.36), custom_call_target="tpu_custom_call" | custom-call | tf_op jit(solution)/shard_map/recurrence/pallas_call | solution.py:355
  153.4 7.8 %fusion.46 = f32[256,4096]{1,0:T(8,128)} fusion(bf16[256,1024]{1,0:T(8,128)(2,1)} %recurrence.1, bf16[1024,4096]{1,0:T(8,128)(2,1)} %param.29), kind=kOutput, calls=%fused_computation.62 | convolution fusion | flops 2147483648 | bytes 13107200 | tf_op jit(solution)/shard_map/dot_general | solution.py:472
  161.2 45.3 %final.1 = (bf16[64,4096]{1,0:T(8,128)(2,1)}, bf16[64,4096]{1,0:T(8,128)(2,1)}) custom-call(f32[4,64,4096]{2,1,0:T(8,128)} %bitcast.29, f32[4,64,4096]{2,1,0:T(8,128)} %bitcast.26, f32[1,4096]{1,0:T(1,128)} %bitcast.34, f32[1,4096]{1,0:T(1,128)} %bitcast.35), custom_call_target="tpu_custom_call" | custom-call | tf_op jit(solution)/shard_map/final/pallas_call | solution.py:410
  206.5 1.9 copy.28
  208.4 1.9 copy.29
  (17 shorter events, 0.1 us)
Async XLA Ops:
  0.6 114.2 %copy-start = (bf16[256,4096]{1,0:T(8,128)(2,1)S(1)}, bf16[256,4096]{1,0:T(8,128)(2,1)}, u32[]{:S(2)}) copy-start(bf16[256,4096]{1,0:T(8,128)(2,1)} %param.40) | copy-start | bytes 6291460
  0.6 4.0 %copy-start.5 = (f32[4096]{0:T(1024)S(1)}, f32[4096]{0:T(1024)}, u32[]{:S(2)}) copy-start(f32[4096]{0:T(1024)} %param.32) | copy-start | bytes 49156
  2.4 2.3 %copy-start.3 = (bf16[256,4096]{1,0:T(8,128)(2,1)S(1)}, bf16[256,4096]{1,0:T(8,128)(2,1)}, u32[]{:S(2)}) copy-start(bf16[256,4096]{1,0:T(8,128)(2,1)} %param.31) | copy-start | bytes 6291460
  5.3 1.3 copy-start.1
  8.6 101.8 %copy-start.7 = (f32[256,2]{0,1:T(2,128)S(1)}, f32[256,2]{0,1:T(2,128)}, u32[]{:S(2)}) copy-start(f32[256,2]{0,1:T(2,128)} %param.34) | copy-start | bytes 6148
  110.3 2.2 %copy-start.2 = (bf16[256,4096]{1,0:T(8,128)(2,1)S(1)}, bf16[256,4096]{1,0:T(8,128)(2,1)}, u32[]{:S(2)}) copy-start(bf16[256,4096]{1,0:T(8,128)(2,1)} %copy-done.1) | copy-start | bytes 6291460
  121.4 3.5 %copy-start.4 = (bf16[256,4096]{1,0:T(8,128)(2,1)S(1)}, bf16[256,4096]{1,0:T(8,128)(2,1)}, u32[]{:S(2)}) copy-start(bf16[256,4096]{1,0:T(8,128)(2,1)} %param.21) | copy-start | bytes 6291460
  124.9 0.7 copy-start.8
  124.9 8.0 %slice-start = ((s8[8388608]{0:T(1024)(128)(4,1)}), s8[4194304]{0:T(1024)(128)(4,1)S(1)}, s32[]{:S(2)}) async-start(s8[8388608]{0:T(1024)(128)(4,1)} %bitcast.43), calls=%async_computation | async-start | bytes 8388608
  125.6 7.3 %slice-start.1 = ((s8[8388608]{0:T(1024)(128)(4,1)}), s8[4194304]{0:T(1024)(128)(4,1)S(1)}, s32[]{:S(2)}) async-start(s8[8388608]{0:T(1024)(128)(4,1)} %bitcast.43), calls=%async_computation.1 | async-start | bytes 8388608
  132.9 3.3 %copy-start.6 = (f32[1024]{0:T(1024)S(1)}, f32[1024]{0:T(1024)}, u32[]{:S(2)}) copy-start(f32[1024]{0:T(1024)} %param.28) | copy-start | bytes 12292

commit v2 on v1

v2 whole, which is shorter than its diff:
```python
import functools

import jax
import jax.numpy as jnp
from jax import lax
from jax.experimental import pallas as pl
from jax.experimental.pallas import tpu as pltpu
from jax.sharding import PartitionSpec as P

eps = 1e-06
lru_power = 8.0
halo_rows = 16
MESH = pl.DeviceIdType.MESH
f32 = jnp.float32
bf16 = jnp.bfloat16


def rms_scale(values, scale):
    floats = values.astype(f32)
    return floats * lax.rsqrt(jnp.mean(floats * floats, axis=-1, keepdims=True) + eps) * scale


def remote(src, dst, send_sem, recv_sem, ep_at, tp_at):
    return pltpu.make_async_remote_copy(
        src_ref=src,
        dst_ref=dst,
        send_sem=send_sem,
        recv_sem=recv_sem,
        device_id=(ep_at, tp_at),
        device_id_type=MESH,
    )


def greet(peers):
    barrier = pltpu.get_barrier_semaphore()
    for ep_at, tp_at in peers:
        pl.semaphore_signal(barrier, inc=1, device_id=(ep_at, tp_at), device_id_type=MESH)
    pl.semaphore_wait(barrier, len(peers))


def expm1_neg(y):
    series = y * (1 + y / 2 * (1 + y / 3 * (1 + y / 4 * (1 + y / 5 * (1 + y / 6 * (1 + y / 7))))))
    return jnp.where(y > -0.35, series, jnp.exp(y) - 1.0)


def layer_kernel(
    ep, tp, top,
    outq, normed, en, taps_ref, ig_ref, dg_ref, soft_ref, picks, weights, ms_ref, es_ref,
    ip_hbm, gp_hbm, op_hbm, eg_hbm, eu_hbm, ed, sg_hbm, su_hbm, sd_hbm,
    mo_ref, eo_ref,
    w1, eg, eu, wd, sd, recv, hid, ret, back, mt, st, m_half, e_half, m_out, m_in, e_in,
    r_buf, r_in, total, gate, a_buf, b_buf, ext, tail, halo, ends, got, gated,
    load_sem, halo_send, halo_recv, end_send, end_recv,
    z_s, z_r, y_s, y_r, c_s, c_r, hy_s, hy_r, hc_s, hc_r, w_s, w_r, b_s, b_r,
    md_s, md_r, ed_s, ed_r, my_s, my_r, ey_s, ey_r, r_s, r_r,
):
    me, t = lax.axis_index("ep"), lax.axis_index("tp")
    ys = tp // 2
    y, c = t // 2, lax.rem(t, 2)
    mate = y * 2 + 1 - c
    dq = outq.shape[2]
    rows, width = ext.shape[0] - halo_rows, ext.shape[1]
    each = rows // tp
    blocks, bw = ig_ref.shape[0], ig_ref.shape[1]
    sh_width = sd.shape[0]

    def at_y(k):
        return lax.rem(y + k, ys)

    def up(k):
        return at_y(k) * 2 + c

    def down_of(k, core):
        return lax.rem(y + ys - k, ys) * 2 + core

    greet(
        [(lax.rem(me + i, ep), t) for i in range(1, ep)]
        + [(me, lax.rem(t + i, tp)) for i in range(1, tp)]
    )

    def z_copy(i):
        return remote(
            outq.at[i], recv.at[t, i], z_s.at[i], z_r.at[i], lax.rem(me + i, ep), t
        )

    def y_copy(k, i):
        return remote(recv.at[t, i], recv.at[t, i], y_s.at[k, i], y_r.at[k, i], me, up(k))

    def c_copy(k, i):
        q = down_of(k, c)
        return remote(recv.at[q, i], recv.at[q, i], c_s.at[k, i], c_r.at[k, i], me, mate)

    def hy_copy(k, i):
        return remote(hid.at[t, i], hid.at[t, i], hy_s.at[k, i], hy_r.at[k, i], me, up(k))

    def hc_copy(k, i):
        q = down_of(k, c)
        return remote(hid.at[q, i], hid.at[q, i], hc_s.at[k, i], hc_r.at[k, i], me, mate)

    def w_copy(i):
        q = lax.rem(t + i, tp)
        return remote(
            ed.at[:, pl.ds(pl.multiple_of(q * dq, dq), dq)], wd.at[t],
            w_s.at[i], w_r.at[i], me, q,
        )

    def b_copy(i):
        return remote(
            ret.at[i], back.at[i], b_s.at[i], b_r.at[i], lax.rem(me + ep - i, ep), t
        )

    def halo_copy():
        return remote(tail, halo, halo_send, halo_recv, lax.rem(me + 1, ep), t)

    def end_copy(i):
        return remote(ends, got.at[i], end_send.at[i], end_recv.at[i], lax.rem(me + i, ep), t)

    def pair(ref, half, s, r, k):
        return remote(ref.at[at_y(k) * 2 + 1 - c], half.at[k], s.at[k], r.at[k], me, mate)

    def my_copy(k):
        return remote(m_out.at[k], m_in.at[k], my_s.at[k], my_r.at[k], me, up(k))

    def ey_copy(k):
        return remote(e_half.at[k], e_in.at[k], ey_s.at[k], ey_r.at[k], me, up(k))

    def r_copy(i):
        q = lax.rem(t + i, tp)
        return remote(r_buf.at[q], r_in.at[t], r_s.at[i], r_r.at[i], me, q)

    def load(src, dst, at):
        return pltpu.make_async_copy(src, dst, load_sem.at[at])

    for i in range(1, ep):
        z_copy(i).start()
    own_rows = load(outq.at[0], recv.at[t, 0], 0)
    own_rows.start()
    ip_load = load(ip_hbm, w1, 1)
    ip_load.start()
    eg_load, eu_load = load(eg_hbm, eg, 2), load(eu_hbm, eu, 3)
    eg_load.start()
    eu_load.start()
    wd_load = load(ed.at[:, pl.ds(pl.multiple_of(t * dq, dq), dq)], wd.at[t], 4)
    wd_load.start()
    sd_load = load(sd_hbm, sd, 5)
    sd_load.start()
    sg_load = load(sg_hbm, w1.at[:, pl.ds(0, sh_width)], 6)
    su_load = load(su_hbm, w1.at[:, pl.ds(sh_width, sh_width)], 7)
    gp_load = load(gp_hbm, w1, 8)
    op_loads = [
        load(op_hbm.at[:, pl.ds(q * dq, dq)], w1.at[pl.ds(q * width, width), :], 9 + q)
        for q in range(tp)
    ]
    own_rows.wait()

    def project():
        ip_load.wait()

        def columns(j, _):
            cols = pl.ds(pl.multiple_of(j * bw, bw), bw)
            piece = jnp.dot(normed[...], w1[:, cols], preferred_element_type=f32).astype(bf16)
            ext[pl.ds(halo_rows, rows), cols] = piece.astype(f32)
            tail[:, cols] = piece[rows - halo_rows :]
            return 0

        lax.fori_loop(0, width // bw, columns, 0)
        halo_copy().start()
        sg_load.start()
        su_load.start()

    def shared():
        sg_load.wait()
        su_load.wait()
        g = jnp.dot(en[...], w1[:, pl.ds(0, sh_width)], preferred_element_type=f32)
        u = jnp.dot(en[...], w1[:, pl.ds(sh_width, sh_width)], preferred_element_type=f32)
        hidden = (jax.nn.silu(g) * u).astype(bf16)
        gp_load.start()
        sd_load.wait()
        for q in range(tp):
            cols = pl.ds(q * dq, dq)
            piece = jnp.dot(hidden, sd[:, cols], preferred_element_type=f32)
            st[:, :, cols] = piece.reshape(tp, each, dq)

    def gate_step():
        gp_load.wait()

        def columns(j, _):
            cols = pl.ds(pl.multiple_of(j * bw, bw), bw)
            piece = jnp.dot(normed[...], w1[:, cols], preferred_element_type=f32)
            gate[:, cols] = jax.nn.gelu(piece)
            return 0

        lax.fori_loop(0, width // bw, columns, 0)
        for one in op_loads:
            one.start()

    def convolve():
        halo_copy().wait()
        ext[pl.ds(0, halo_rows), :] = jnp.where(me == 0, 0.0, halo[...].astype(f32))
        taps = taps_ref.shape[0]
        base = halo_rows - (taps - 1)
        first = (lax.broadcasted_iota(jnp.int32, (rows, bw), 0) == 0) & (me == 0)
        for b in range(blocks):
            cols = pl.ds(b * bw, bw)
            acc = taps_ref[0:1, cols] * ext[pl.ds(base, rows), cols]
            for k in range(1, taps):
                acc = acc + taps_ref[k : k + 1, cols] * ext[pl.ds(base + k, rows), cols]
            conv = acc.astype(bf16)
            ig = jax.nn.sigmoid(jnp.dot(conv, ig_ref[b], preferred_element_type=f32))
            dg = jax.nn.sigmoid(jnp.dot(conv, dg_ref[b], preferred_element_type=f32))
            ld = -lru_power * dg * soft_ref[0:1, cols]
            scale = jnp.where(first, 1.0, jnp.sqrt(-expm1_neg(2.0 * ld)))
            a_buf[:, cols] = jnp.exp(ld)
            b_buf[:, cols] = scale * ig * conv.astype(f32)

    def scan():
        row = lax.broadcasted_iota(jnp.int32, (8, width), 0)

        def block(r, carry):
            pc, sc = carry
            at = pl.ds(pl.multiple_of(r * 8, 8), 8)
            a, b = a_buf[at, :], b_buf[at, :]
            for sh in (1, 2, 4):
                keep = row >= sh
                b = jnp.where(keep, b + a * pltpu.roll(b, sh, 0), b)
                a = jnp.where(keep, a * pltpu.roll(a, sh, 0), a)
            b = b + a * sc
            a = a * pc
            a_buf[at, :] = a
            b_buf[at, :] = b
            return a[7:8, :], b[7:8, :]

        pl_last, s_last = lax.fori_loop(
            0, rows // 8, block, (jnp.ones((1, width), f32), jnp.zeros((1, width), f32))
        )
        ends[...] = jnp.where(row == 0, pl_last, s_last)
        for i in range(1, ep):
            end_copy(i).start()

    def carry_in():
        for i in range(1, ep):
            end_copy(i).wait()
        carry = jnp.zeros((1, width), f32)
        for i in range(ep - 1, 0, -1):
            carry = jnp.where(me >= i, got[i, 0:1, :] * carry + got[i, 1:2, :], carry)

        def finish(r, _):
            at = pl.ds(pl.multiple_of(r * 16, 16), 16)
            gated[at, :] = (gate[at, :] * (b_buf[at, :] + a_buf[at, :] * carry)).astype(bf16)
            return 0

        lax.fori_loop(0, rows // 16, finish, 0)

    def project_out():
        for one in op_loads:
            one.wait()
        for q in range(tp):
            piece = jnp.dot(
                gated[...], w1[pl.ds(q * width, width), :], preferred_element_type=f32
            )
            mt[:, :, pl.ds(q * dq, dq)] = piece.reshape(tp, each, dq)
        for k in range(ys):
            pair(mt, m_half, md_s, md_r, k).start()
        for k in range(ys):
            pair(st, e_half, ed_s, ed_r, k).start()

    def halves():
        for k in range(1, ys):
            pair(mt, m_half, md_s, md_r, k).wait_recv()
            m_out[k] = (m_half[k] + mt[up(k)]).astype(bf16)
            my_copy(k).start()
        for k in range(1, ys):
            pair(st, e_half, ed_s, ed_r, k).wait_recv()
            e_half[k] = e_half[k] + st[up(k)]
            ey_copy(k).start()

    work = {
        0: project, 1: shared, 2: gate_step, 3: convolve, 4: scan, 5: carry_in, 6: project_out,
        ep + 2: halves,
    }

    def step(n, _):
        @pl.when(n < ep)
        def _():
            i = n

            @pl.when(i > 0)
            def _():
                z_copy(i).wait_recv()

            for k in range(1, ys):
                y_copy(k, i).start()
            c_copy(0, i).start()

        @pl.when(n == 1)
        def _():
            for i in range(1, tp):
                w_copy(i).start()

        @pl.when((n >= 1) & (n < ep + 1))
        def _():
            i = n - 1
            for k in range(1, ys):
                y_copy(k, i).wait_recv()
                c_copy(k, i).start()

        @pl.when(n == 2)
        def _():
            eg_load.wait()
            eu_load.wait()

        @pl.when((n >= 2) & (n < ep + 2))
        def _():
            i = n - 2
            for k in range(ys):
                c_copy(k, i).wait_recv()
            gate_sum = up_sum = None
            for q in range(tp):
                x = recv[q, i]
                span = pl.ds(q * dq, dq)
                g = jnp.dot(x, eg[span, :], preferred_element_type=f32)
                u = jnp.dot(x, eu[span, :], preferred_element_type=f32)
                gate_sum = g if gate_sum is None else gate_sum + g
                up_sum = u if up_sum is None else up_sum + u
            hid[t, i] = (jax.nn.silu(gate_sum) * up_sum).astype(bf16)
            for k in range(1, ys):
                hy_copy(k, i).start()
            hc_copy(0, i).start()

        @pl.when((n >= 3) & (n < ep + 3))
        def _():
            i = n - 3
            for k in range(1, ys):
                hy_copy(k, i).wait_recv()
                hc_copy(k, i).start()

        @pl.when(n == 4)
        def _():
            wd_load.wait()
            for i in range(1, tp):
                w_copy(i).wait()

        @pl.when(n >= 4)
        def _():
            i = n - 4
            for k in range(ys):
                hc_copy(k, i).wait_recv()
            out = jnp.dot(hid[0, i], wd[0], preferred_element_type=f32)
            for q in range(1, tp):
                out = out + jnp.dot(hid[q, i], wd[q], preferred_element_type=f32)

            @pl.when(i == 0)
            def _():
                back[0] = out.astype(bf16)

            @pl.when(i > 0)
            def _():
                ret[i] = out.astype(bf16)
                b_copy(i).start()

        for at, task in work.items():
            pl.when(n == at)(task)
        return 0

    lax.fori_loop(0, ep + 4, step, 0)

    pair(mt, m_half, md_s, md_r, 0).wait_recv()
    whole = m_half[0] + mt[t]
    for k in range(1, ys):
        my_copy(k).wait_recv()
        whole = whole + m_in[k].astype(f32)
    mo_ref[...] = rms_scale(whole, ms_ref[...]).astype(bf16)
    pair(st, e_half, ed_s, ed_r, 0).wait_recv()
    whole = e_half[0] + st[t]
    for k in range(1, ys):
        ey_copy(k).wait_recv()
        whole = whole + e_in[k]
    total[...] = whole

    def arrive(i, _):
        b_copy(i).wait()
        return 0

    lax.fori_loop(1, ep, arrive, 0)
    flat = back[...].reshape(-1, dq)
    routed = None
    for k in range(top):
        term = weights[:, k : k + 1] * jnp.dot(picks[k], flat, preferred_element_type=f32)
        routed = term if routed is None else routed + term
    r_buf[...] = routed.reshape(tp, each, dq)
    for i in range(1, tp):
        r_copy(i).start()
    mine = pl.ds(pl.multiple_of(t * dq, dq), dq)
    total[:, mine] = total[:, mine] + r_buf[t]
    for i in range(1, tp):
        r_copy(i).wait()
        q = lax.rem(t + tp - i, tp)
        cols = pl.ds(pl.multiple_of(q * dq, dq), dq)
        total[:, cols] = total[:, cols] + r_in[q]
    eo_ref[...] = rms_scale(total[...], es_ref[...]).astype(bf16)

    def settle(i, _):
        for k in range(1, ys):
            y_copy(k, i).wait_send()
            hy_copy(k, i).wait_send()
        for k in range(ys):
            c_copy(k, i).wait_send()
            hc_copy(k, i).wait_send()

        @pl.when(i > 0)
        def _():
            z_copy(i).wait_send()

        return 0

    lax.fori_loop(0, ep, settle, 0)
    for k in range(ys):
        pair(mt, m_half, md_s, md_r, k).wait_send()
        pair(st, e_half, ed_s, ed_r, k).wait_send()
    for k in range(1, ys):
        my_copy(k).wait_send()
        ey_copy(k).wait_send()


def dma(*shape):
    return pltpu.SemaphoreType.DMA(shape)


def layer(ep, tp, small, large):
    outq, normed, _, _, ig = small[:5]
    picks = small[7]
    _, cap, dq = outq.shape
    rows, depth = normed.shape
    width = large[0].shape[1]
    hf, hs = large[3].shape[1], large[6].shape[1]
    each, ys, top = rows // tp, tp // 2, picks.shape[0]
    V = pltpu.VMEM
    return pl.pallas_call(
        functools.partial(layer_kernel, ep, tp, top),
        out_shape=[jax.ShapeDtypeStruct((each, depth), bf16)] * 2,
        in_specs=[pl.BlockSpec(memory_space=V)] * len(small)
        + [pl.BlockSpec(memory_space=pl.ANY)] * len(large),
        out_specs=[pl.BlockSpec(memory_space=V)] * 2,
        scratch_shapes=[
            V((depth, width), bf16),
            V((depth, hf), bf16),
            V((depth, hf), bf16),
            V((tp, hf, dq), bf16),
            V((hs, depth), bf16),
            V((tp, ep, cap, dq), bf16),
            V((tp, ep, cap, hf), bf16),
            V((ep, cap, dq), bf16),
            V((ep, cap, dq), bf16),
            V((tp, each, depth), f32),
            V((tp, each, depth), f32),
            V((ys, each, depth), f32),
            V((ys, each, depth), f32),
            V((ys, each, depth), bf16),
            V((ys, each, depth), bf16),
            V((ys, each, depth), f32),
            V((tp, each, dq), f32),
            V((tp, each, dq), f32),
            V((each, depth), f32),
            V((rows, width), f32),
            V((rows, width), f32),
            V((rows, width), f32),
            V((halo_rows + rows, width), f32),
            V((halo_rows, width), bf16),
            V((halo_rows, width), bf16),
            V((8, width), f32),
            V((ep, 8, width), f32),
            V((rows, width), bf16),
            dma(9 + tp), pltpu.SemaphoreType.DMA, pltpu.SemaphoreType.DMA, dma(ep), dma(ep),
            dma(ep), dma(ep),
            dma(ys, ep), dma(ys, ep),
            dma(ys, ep), dma(ys, ep),
            dma(ys, ep), dma(ys, ep),
            dma(ys, ep), dma(ys, ep),
            dma(tp), dma(tp),
            dma(ep), dma(ep),
            dma(ys), dma(ys), dma(ys), dma(ys),
            dma(ys), dma(ys), dma(ys), dma(ys),
            dma(tp), dma(tp),
        ],
        compiler_params=pltpu.CompilerParams(
            collective_id=0, has_side_effects=True, vmem_limit_bytes=67000000
        ),
        name="layer",
    )(*small, *large)


def body(
    mixer_rows, mixer_gain, gate_proj, input_proj, conv_taps, input_gates, decay_gates,
    decay_offset, out_proj, mixer_scale, expert_rows, expert_gain, route_ids, route_weights,
    expert_gate, expert_up, expert_down, shared_gate, shared_up, shared_down, expert_scale,
):
    ep, tp = lax.axis_size("ep"), lax.axis_size("tp")
    me, t = lax.axis_index("ep"), lax.axis_index("tp")
    tokens, width = expert_rows.shape
    top = route_ids.shape[1]
    cap = tokens * top * 3 // (2 * ep)
    dq = width // tp

    expert_normed = rms_scale(expert_rows, expert_gain).astype(bf16)
    offset_ids = lax.rem(route_ids + (ep - me), ep)
    indicator = jnp.sum(
        (offset_ids[:, :, None] == jnp.arange(ep, dtype=jnp.int32)).astype(f32), axis=1
    )
    below = (
        jnp.arange(tokens)[:, None] > jnp.arange(tokens)[None, :]
    ).astype(bf16)
    earlier = jnp.dot(below, indicator.astype(bf16), preferred_element_type=f32)
    chosen = (offset_ids[:, :, None] == jnp.arange(ep, dtype=jnp.int32)).astype(f32)
    position = jnp.sum(chosen * earlier[:, None, :], axis=2).astype(jnp.int32)
    slot_ids = offset_ids * cap + position
    slots = jnp.arange(ep * cap, dtype=jnp.int32)
    picks = [(slot_ids[:, k][:, None] == slots[None, :]).astype(bf16) for k in range(top)]
    placed = sum(picks[1:], picks[0])
    quarter = lax.dynamic_slice_in_dim(expert_normed, t * dq, dq, axis=1)
    outq = lax.dot_general(
        placed, quarter, (((0,), (0,)), ((), ())), preferred_element_type=f32
    ).astype(bf16).reshape(ep, cap, dq)
    normed = rms_scale(mixer_rows, mixer_gain).astype(bf16)
    soft = jax.nn.softplus(-decay_offset).reshape(1, -1)
    small = (
        outq, normed, expert_normed, conv_taps, input_gates, decay_gates, soft, jnp.stack(picks),
        route_weights, mixer_scale.reshape(1, -1), expert_scale.reshape(1, -1),
    )
    large = (
        input_proj, gate_proj, out_proj, expert_gate[0], expert_up[0], expert_down[0],
        shared_gate, shared_up, shared_down,
    )
    return tuple(layer(ep, tp, small, large))


def solution(mesh):
    placed = (
        P("ep", None),
        P(),
        P(None, "tp"),
        P(None, "tp"),
        P(None, "tp"),
        P("tp", None, None),
        P("tp", None, None),
        P("tp"),
        P("tp", None),
        P(),
        P("ep", None),
        P(),
        P("ep", None),
        P("ep", None),
        P("ep", None, "tp"),
        P("ep", None, "tp"),
        P("ep", "tp", None),
        P(None, "tp"),
        P(None, "tp"),
        P("tp", None),
        P(),
    )
    return jax.shard_map(
        body,
        mesh=mesh,
        in_specs=placed,
        out_specs=(P(("ep", "tp"), None), P(("ep", "tp"), None)),
        check_vma=False,
    )
```

time: 211 us -> 155 us (0.73); the launches traced: 210 us -> 152 us
  matrix products: 35 us -> 2.08 us
  Pallas kernels: 164 us -> 134 us
  other arithmetic: 5.58 us -> 8.97 us
    dot_general x7 -> x0, matrix products: 32.9 us -> none  [the longest x1 7.84 us: body(): mixer_term = jnp.dot(gated, out_proj, preferred_element_type=f32)]
    pallas_call x3 -> x1, Pallas kernels: 164 us -> 134 us  [layer(): pl.pallas_call(functools.partial(layer_kernel, ep, tp, top), out_shape=[j...]
    convert_element_type x1, other arithmetic: 0.64 us -> 4.3 us  [body(): expert_normed = rms_scale(expert_rows, expert_gain).astype(bf16)]
    unnamed x24 -> x17, local copies, waits for them, and re-layouts: 5.31 us -> 5.86 us
where the time goes in v2:
time: 155 us; the launch traced here: 152 us
  Pallas kernels  134 us (86%)
  other arithmetic  8.97 us (6%)
  local copies, waits for them, and re-layouts  5.86 us (4%)
  matrix products  2.08 us (1%)
    pallas_call x1, Pallas kernels, layer(): pl.pallas_call(functools.partial(layer_kernel, ep, tp, top), out_shape=[j...  134 us
    unnamed x17, local copies, waits for them, and re-layouts  5.86 us
    convert_element_type x1, other arithmetic, body(): expert_normed = rms_scale(expert_rows, expert_gain).astype(bf16)  4.3 us

profile of v2, /device:TPU:1, one launch (start us, length us, event | category | flops | bytes accessed | tf_op | source)
XLA Modules:
  0.0 152.0 jit_solution(2470065533477472231)
XLA Ops:
  0.6 0.0 copy-start.1
  0.6 0.0 copy-start.4
  0.7 0.0 copy-start.5
  0.7 0.0 copy-start.6
  0.7 2.2 %fusion.3 = f32[256]{0:T(256)S(1)} fusion(bf16[256,4096]{1,0:T(8,128)(2,1)} %param.21), kind=kLoop, calls=%fused_computation.7 | loop fusion | flops 3145472 | bytes 2098176 | tf_op jit(solution)/shard_map/reduce_sum | solution.py:20
  2.9 0.0 copy-start.2
  2.9 0.0 copy-start.3
  2.9 0.0 copy-done.1
  2.9 0.5 fusion
  3.4 0.0 copy-done.4
  3.5 0.2 fusion.14
  3.7 0.0 copy-done.5
  3.7 0.6 compare_select_fusion
  4.3 0.0 copy-done.6
  4.3 0.8 copy.26.weights
  5.1 0.3 iota_compare_fusion
  5.4 1.0 add_convert_fusion.picks
  6.4 0.0 copy-done.2
  6.4 0.0 copy-done.3
  6.4 4.3 %fusion.2 = (bf16[256,4096]{1,0:T(8,128)(2,1)S(1)}, bf16[256,4096]{1,0:T(8,128)(2,1)}) fusion(bf16[256,4096]{1,0:T(8,128)(2,1)S(1)} %copy-done.1, f32[4096]{0:T(1024)S(1)} %copy-done.2, f32[256]{0:T(256)S(1)} %add_rsqrt_fusion.1, f32[4096]{0:T(1024)S(1)} %copy-done.3, f32[256]{0:T(256)S(1)} %add_rsqrt_fusion, bf16[256,4096]{1,0:T(8,128)(2,1)} %param.21), kind=kLoop, calls=%fused_computation.6 | loop fusion | flops 8388608 | bytes 8423424 | tf_op jit(solution)/shard_map/convert_element_type | solution.py:504
  10.7 0.0 copy-start
  10.7 1.3 copy-done
  12.0 1.9 %convolution_convert_fusion = bf16[768,1024]{1,0:T(8,128)(2,1)} fusion(bf16[256,4096]{1,0:T(8,128)(2,1)S(1)} %get-tuple-element.6.en, s32[]{:T(128)S(6)} %select_n.7, s32[256]{0:T(256)S(1)} %bitcast.20, s32[256]{0:T(256)S(1)} %bitcast.18), kind=kOutput, calls=%fused_computation.10 | convolution fusion | flops 405012480 | bytes 2099204 | tf_op jit(solution)/shard_map/dot_general | solution.py:520
  13.9 134.3 %layer.1 = (bf16[64,4096]{1,0:T(8,128)(2,1)}, bf16[64,4096]{1,0:T(8,128)(2,1)}) custom-call(bf16[8,96,1024]{2,1,0:T(8,128)(2,1)} %bitcast.13, bf16[256,4096]{1,0:T(8,128)(2,1)} %get-tuple-element.7.normed, bf16[256,4096]{1,0:T(8,128)(2,1)} %copy-done, f32[4,1024]{1,0:T(4,128)} %taps_ref.1, bf16[4,256,256]{2,1,0:T(8,128)(2,1)} %ig_ref.1, ...), custom_call_target="tpu_custom_call" | custom-call | tf_op jit(solution)/shard_map/layer/pallas_call | solution.py:438
  148.2 1.9 %copy.29 = bf16[64,4096]{1,0:T(8,128)(2,1)} copy(bf16[64,4096]{1,0:T(8,128)(2,1)} %get-tuple-element.10) | data formatting | bytes 1048576
  150.1 1.9 %copy.30 = bf16[64,4096]{1,0:T(8,128)(2,1)} copy(bf16[64,4096]{1,0:T(8,128)(2,1)} %get-tuple-element.11) | data formatting | bytes 1048576
  (7 shorter events, 0.1 us)
Async XLA Ops:
  0.6 2.3 %copy-start.1 = (bf16[256,4096]{1,0:T(8,128)(2,1)S(1)}, bf16[256,4096]{1,0:T(8,128)(2,1)}, u32[]{:S(2)}) copy-start(bf16[256,4096]{1,0:T(8,128)(2,1)} %param.31) | copy-start | bytes 6291460
  0.6 2.8 %copy-start.4 = (s32[256,2]{0,1:T(2,128)S(1)}, s32[256,2]{0,1:T(2,128)}, u32[]{:S(2)}) copy-start(s32[256,2]{0,1:T(2,128)} %param.33) | copy-start | bytes 6148
  0.7 3.1 %copy-start.5 = (f32[1024]{0:T(1024)S(1)}, f32[1024]{0:T(1024)}, u32[]{:S(2)}) copy-start(f32[1024]{0:T(1024)} %param.28) | copy-start | bytes 12292
  0.7 3.7 %copy-start.6 = (f32[256,2]{0,1:T(2,128)S(1)}, f32[256,2]{0,1:T(2,128)}, u32[]{:S(2)}) copy-start(f32[256,2]{0,1:T(2,128)} %param.34) | copy-start | bytes 6148
  2.9 3.5 %copy-start.2 = (f32[4096]{0:T(1024)S(1)}, f32[4096]{0:T(1024)}, u32[]{:S(2)}) copy-start(f32[4096]{0:T(1024)} %param.32) | copy-start | bytes 49156
  2.9 3.5 %copy-start.3 = (f32[4096]{0:T(1024)S(1)}, f32[4096]{0:T(1024)}, u32[]{:S(2)}) copy-start(f32[4096]{0:T(1024)} %param.22) | copy-start | bytes 49156
  10.7 1.3 copy-start

commit v3 on v2

--- a/solution.py
+++ b/solution.py
@@ -45,9 +45,10 @@
 
 def layer_kernel(
     ep, tp, top,
-    outq, normed, en, taps_ref, ig_ref, dg_ref, soft_ref, picks, weights, ms_ref, es_ref,
-    ip_hbm, gp_hbm, op_hbm, eg_hbm, eu_hbm, ed, sg_hbm, su_hbm, sd_hbm,
+    slots, slots_t, taps_ref, ig_ref, dg_ref, soft_ref, weights, mg_ref, xg_ref, ms_ref, es_ref,
+    rows_hbm, tokens_hbm, ip_hbm, gp_hbm, op_hbm, eg_hbm, eu_hbm, ed, sg_hbm, su_hbm, sd_hbm,
     mo_ref, eo_ref,
+    outq, normed, en, e_out, r_out, r_near,
     w1, eg, eu, wd, sd, recv, hid, ret, back, mt, st, m_half, e_half, m_out, m_in, e_in,
     r_buf, r_in, total, gate, a_buf, b_buf, ext, tail, halo, ends, got, gated,
     load_sem, halo_send, halo_recv, end_send, end_recv,
@@ -122,19 +123,22 @@
         return remote(m_out.at[k], m_in.at[k], my_s.at[k], my_r.at[k], me, up(k))
 
     def ey_copy(k):
-        return remote(e_half.at[k], e_in.at[k], ey_s.at[k], ey_r.at[k], me, up(k))
-
-    def r_copy(i):
-        q = lax.rem(t + i, tp)
-        return remote(r_buf.at[q], r_in.at[t], r_s.at[i], r_r.at[i], me, q)
+        return remote(e_out.at[k], e_in.at[k], ey_s.at[k], ey_r.at[k], me, up(k))
+
+    def r_copy(k, core):
+        j, q = 2 * k + core, at_y(k) * 2 + lax.rem(c + core, 2)
+        if k == 0:
+            return remote(r_buf.at[q], r_near, r_s.at[j], r_r.at[j], me, q)
+        return remote(r_out.at[q], r_in.at[t], r_s.at[j], r_r.at[j], me, q)
 
     def load(src, dst, at):
         return pltpu.make_async_copy(src, dst, load_sem.at[at])
 
-    for i in range(1, ep):
-        z_copy(i).start()
-    own_rows = load(outq.at[0], recv.at[t, 0], 0)
-    own_rows.start()
+    for i in range(1, tp):
+        w_copy(i).start()
+    tokens_load, rows_load = load(tokens_hbm, en, 0), load(rows_hbm, normed, 9 + tp)
+    tokens_load.start()
+    rows_load.start()
     ip_load = load(ip_hbm, w1, 1)
     ip_load.start()
     eg_load, eu_load = load(eg_hbm, eg, 2), load(eu_hbm, eu, 3)
@@ -144,6 +148,40 @@
     wd_load.start()
     sd_load = load(sd_hbm, sd, 5)
     sd_load.start()
+
+    def normalize(ref, gain):
+        def some(r, _):
+            at = pl.ds(pl.multiple_of(r * 32, 32), 32)
+            ref[at, :] = rms_scale(ref[at, :], gain[...]).astype(bf16)
+            return 0
+
+        lax.fori_loop(0, rows // 32, some, 0)
+
+    tokens_load.wait()
+    normalize(en, xg_ref)
+    cap = outq.shape[1]
+    mine = pl.ds(pl.multiple_of(t * dq, dq), dq)
+
+    def place(i):
+        spot = lax.broadcasted_iota(jnp.int32, (cap, rows), 0) + i * cap
+        hot = slots_t[0:1, :] == spot
+        for k in range(1, top):
+            hot = hot | (slots_t[k : k + 1, :] == spot)
+        return hot.astype(f32).astype(bf16)
+
+    def dispatch(i, _):
+        outq[i] = jnp.dot(place(i), en[:, mine], preferred_element_type=f32).astype(bf16)
+        z_copy(i).start()
+        return 0
+
+    lax.fori_loop(1, ep, dispatch, 0)
+    local = place(0)
+    for q in range(tp):
+        recv[q, 0] = jnp.dot(
+            local, en[:, pl.ds(q * dq, dq)], preferred_element_type=f32
+        ).astype(bf16)
+    rows_load.wait()
+    normalize(normed, mg_ref)
     sg_load = load(sg_hbm, w1.at[:, pl.ds(0, sh_width)], 6)
     su_load = load(su_hbm, w1.at[:, pl.ds(sh_width, sh_width)], 7)
     gp_load = load(gp_hbm, w1, 8)
@@ -151,7 +189,6 @@
         load(op_hbm.at[:, pl.ds(q * dq, dq)], w1.at[pl.ds(q * width, width), :], 9 + q)
         for q in range(tp)
     ]
-    own_rows.wait()
 
     def project():
         ip_load.wait()
@@ -180,6 +217,8 @@
             cols = pl.ds(q * dq, dq)
             piece = jnp.dot(hidden, sd[:, cols], preferred_element_type=f32)
             st[:, :, cols] = piece.reshape(tp, each, dq)
+        for k in range(ys):
+            pair(st, e_half, ed_s, ed_r, k).start()
 
     def gate_step():
         gp_load.wait()
@@ -261,43 +300,34 @@
             mt[:, :, pl.ds(q * dq, dq)] = piece.reshape(tp, each, dq)
         for k in range(ys):
             pair(mt, m_half, md_s, md_r, k).start()
-        for k in range(ys):
-            pair(st, e_half, ed_s, ed_r, k).start()
-
-    def halves():
+
+    def shared_half():
+        for k in range(1, ys):
+            pair(st, e_half, ed_s, ed_r, k).wait_recv()
+            e_out[k] = (e_half[k] + st[up(k)]).astype(bf16)
+            ey_copy(k).start()
+
+    def mixer_half():
         for k in range(1, ys):
             pair(mt, m_half, md_s, md_r, k).wait_recv()
             m_out[k] = (m_half[k] + mt[up(k)]).astype(bf16)
             my_copy(k).start()
-        for k in range(1, ys):
-            pair(st, e_half, ed_s, ed_r, k).wait_recv()
-            e_half[k] = e_half[k] + st[up(k)]
-            ey_copy(k).start()
 
     work = {
         0: project, 1: shared, 2: gate_step, 3: convolve, 4: scan, 5: carry_in, 6: project_out,
-        ep + 2: halves,
+        ep - 1: shared_half, ep + 2: mixer_half,
     }
 
     def step(n, _):
-        @pl.when(n < ep)
+        @pl.when((n > 0) & (n < ep))
         def _():
             i = n
-
-            @pl.when(i > 0)
-            def _():
-                z_copy(i).wait_recv()
-
+            z_copy(i).wait_recv()
             for k in range(1, ys):
                 y_copy(k, i).start()
             c_copy(0, i).start()
 
-        @pl.when(n == 1)
-        def _():
-            for i in range(1, tp):
-                w_copy(i).start()
-
-        @pl.when((n >= 1) & (n < ep + 1))
+        @pl.when((n >= 2) & (n < ep + 1))
         def _():
             i = n - 1
             for k in range(1, ys):
@@ -312,8 +342,12 @@
         @pl.when((n >= 2) & (n < ep + 2))
         def _():
             i = n - 2
-            for k in range(ys):
-                c_copy(k, i).wait_recv()
+
+            @pl.when(i > 0)
+            def _():
+                for k in range(ys):
+                    c_copy(k, i).wait_recv()
+
             gate_sum = up_sum = None
             for q in range(tp):
                 x = recv[q, i]
@@ -374,7 +408,7 @@
     whole = e_half[0] + st[t]
     for k in range(1, ys):
         ey_copy(k).wait_recv()
-        whole = whole + e_in[k]
+        whole = whole + e_in[k].astype(f32)
     total[...] = whole
 
     def arrive(i, _):
@@ -383,32 +417,43 @@
 
     lax.fori_loop(1, ep, arrive, 0)
     flat = back[...].reshape(-1, dq)
+    spot = lax.broadcasted_iota(jnp.int32, (rows, ep * cap), 1)
     routed = None
     for k in range(top):
-        term = weights[:, k : k + 1] * jnp.dot(picks[k], flat, preferred_element_type=f32)
+        pick = (slots[:, k : k + 1] == spot).astype(f32).astype(bf16)
+        term = weights[:, k : k + 1] * jnp.dot(pick, flat, preferred_element_type=f32)
         routed = term if routed is None else routed + term
-    r_buf[...] = routed.reshape(tp, each, dq)
-    for i in range(1, tp):
-        r_copy(i).start()
-    mine = pl.ds(pl.multiple_of(t * dq, dq), dq)
+    routed = routed.reshape(tp, each, dq)
+    r_out[...] = routed.astype(bf16)
+    for k in range(1, ys):
+        for core in range(2):
+            r_copy(k, core).start()
+    r_buf[...] = routed
+    r_copy(0, 1).start()
     total[:, mine] = total[:, mine] + r_buf[t]
-    for i in range(1, tp):
-        r_copy(i).wait()
-        q = lax.rem(t + tp - i, tp)
-        cols = pl.ds(pl.multiple_of(q * dq, dq), dq)
-        total[:, cols] = total[:, cols] + r_in[q]
+    r_copy(0, 1).wait()
+    near = pl.ds(pl.multiple_of(mate * dq, dq), dq)
+    total[:, near] = total[:, near] + r_near[...]
+    for k in range(1, ys):
+        for core in range(2):
+            r_copy(k, core).wait()
+            q = down_of(k, lax.rem(c + core, 2))
+            cols = pl.ds(pl.multiple_of(q * dq, dq), dq)
+            total[:, cols] = total[:, cols] + r_in[q].astype(f32)
     eo_ref[...] = rms_scale(total[...], es_ref[...]).astype(bf16)
 
     def settle(i, _):
         for k in range(1, ys):
-            y_copy(k, i).wait_send()
             hy_copy(k, i).wait_send()
         for k in range(ys):
-            c_copy(k, i).wait_send()
             hc_copy(k, i).wait_send()
 
         @pl.when(i > 0)
         def _():
+            for k in range(1, ys):
+                y_copy(k, i).wait_send()
+            for k in range(ys):
+                c_copy(k, i).wait_send()
             z_copy(i).wait_send()
 
         return 0
@@ -427,13 +472,12 @@
 
 
 def layer(ep, tp, small, large):
-    outq, normed, _, _, ig = small[:5]
-    picks = small[7]
-    _, cap, dq = outq.shape
-    rows, depth = normed.shape
-    width = large[0].shape[1]
-    hf, hs = large[3].shape[1], large[6].shape[1]
-    each, ys, top = rows // tp, tp // 2, picks.shape[0]
+    rows, depth = large[0].shape
+    width = large[2].shape[1]
+    hf, hs = large[5].shape[1], large[8].shape[1]
+    top = small[0].shape[1]
+    each, ys, dq = rows // tp, tp // 2, depth // tp
+    cap = rows * top * 3 // (2 * ep)
     V = pltpu.VMEM
     return pl.pallas_call(
         functools.partial(layer_kernel, ep, tp, top),
@@ -442,6 +486,12 @@
         + [pl.BlockSpec(memory_space=pl.ANY)] * len(large),
         out_specs=[pl.BlockSpec(memory_space=V)] * 2,
         scratch_shapes=[
+            V((ep, cap, dq), bf16),
+            V((rows, depth), bf16),
+            V((rows, depth), bf16),
+            V((ys, each, depth), bf16),
+            V((tp, each, dq), bf16),
+            V((each, dq), f32),
             V((depth, width), bf16),
             V((depth, hf), bf16),
             V((depth, hf), bf16),
@@ -457,9 +507,9 @@
             V((ys, each, depth), f32),
             V((ys, each, depth), bf16),
             V((ys, each, depth), bf16),
-            V((ys, each, depth), f32),
+            V((ys, each, depth), bf16),
             V((tp, each, dq), f32),
-            V((tp, each, dq), f32),
+            V((tp, each, dq), bf16),
             V((each, depth), f32),
             V((rows, width), f32),
             V((rows, width), f32),
@@ -470,7 +520,7 @@
             V((8, width), f32),
             V((ep, 8, width), f32),
             V((rows, width), bf16),
-            dma(9 + tp), pltpu.SemaphoreType.DMA, pltpu.SemaphoreType.DMA, dma(ep), dma(ep),
+            dma(10 + tp), pltpu.SemaphoreType.DMA, pltpu.SemaphoreType.DMA, dma(ep), dma(ep),
             dma(ep), dma(ep),
             dma(ys, ep), dma(ys, ep),
             dma(ys, ep), dma(ys, ep),
@@ -495,13 +545,10 @@
     expert_gate, expert_up, expert_down, shared_gate, shared_up, shared_down, expert_scale,
 ):
     ep, tp = lax.axis_size("ep"), lax.axis_size("tp")
-    me, t = lax.axis_index("ep"), lax.axis_index("tp")
-    tokens, width = expert_rows.shape
+    me = lax.axis_index("ep")
+    tokens = expert_rows.shape[0]
     top = route_ids.shape[1]
     cap = tokens * top * 3 // (2 * ep)
-    dq = width // tp
-
-    expert_normed = rms_scale(expert_rows, expert_gain).astype(bf16)
     offset_ids = lax.rem(route_ids + (ep - me), ep)
     indicator = jnp.sum(
         (offset_ids[:, :, None] == jnp.arange(ep, dtype=jnp.int32)).astype(f32), axis=1
@@ -513,21 +560,13 @@
     chosen = (offset_ids[:, :, None] == jnp.arange(ep, dtype=jnp.int32)).astype(f32)
     position = jnp.sum(chosen * earlier[:, None, :], axis=2).astype(jnp.int32)
     slot_ids = offset_ids * cap + position
-    slots = jnp.arange(ep * cap, dtype=jnp.int32)
-    picks = [(slot_ids[:, k][:, None] == slots[None, :]).astype(bf16) for k in range(top)]
-    placed = sum(picks[1:], picks[0])
-    quarter = lax.dynamic_slice_in_dim(expert_normed, t * dq, dq, axis=1)
-    outq = lax.dot_general(
-        placed, quarter, (((0,), (0,)), ((), ())), preferred_element_type=f32
-    ).astype(bf16).reshape(ep, cap, dq)
-    normed = rms_scale(mixer_rows, mixer_gain).astype(bf16)
     soft = jax.nn.softplus(-decay_offset).reshape(1, -1)
+    gains = [x.reshape(1, -1) for x in (mixer_gain, expert_gain, mixer_scale, expert_scale)]
     small = (
-        outq, normed, expert_normed, conv_taps, input_gates, decay_gates, soft, jnp.stack(picks),
-        route_weights, mixer_scale.reshape(1, -1), expert_scale.reshape(1, -1),
+        slot_ids, slot_ids.T, conv_taps, input_gates, decay_gates, soft, route_weights, *gains,
     )
     large = (
-        input_proj, gate_proj, out_proj, expert_gate[0], expert_up[0], expert_down[0],
+        mixer_rows, expert_rows, input_proj, gate_proj, out_proj, expert_gate[0], expert_up[0], expert_down[0],
         shared_gate, shared_up, shared_down,
     )
     return tuple(layer(ep, tp, small, large))

time: 155 us -> 119 us (0.77); the launches traced: 152 us -> 118 us
  Pallas kernels: 134 us -> 109 us
  other arithmetic: 8.97 us -> 2.74 us
  matrix products: 2.08 us -> 0.15 us
    pallas_call x1, Pallas kernels: 134 us -> 109 us  [layer(): pl.pallas_call(functools.partial(layer_kernel, ep, tp, top), out_shape=[j...]
    convert_element_type x1 -> x0, other arithmetic: 4.3 us -> none  [body(): expert_normed = rms_scale(expert_rows, expert_gain).astype(bf16)]
    reduce_sum x2 -> x0, other arithmetic: 2.72 us -> none  [rms_scale(): jnp.mean(floats * floats, axis=-1, keepdims=True) + eps]
    dot_general x1 -> x0, matrix products: 1.93 us -> none  [body(): lax.dot_general(placed, quarter, (((0,), (0,)), ((), ())), preferred_elem...]
    unnamed x17 -> x5, local copies, waits for them, and re-layouts: 5.86 us -> 5.21 us
where the time goes in v3:
time: 119 us; the launch traced here: 118 us
  Pallas kernels  109 us (92%)
  local copies, waits for them, and re-layouts  6.01 us (5%)
  other arithmetic  2.74 us (2%)
    pallas_call x1, Pallas kernels, layer(): pl.pallas_call(functools.partial(layer_kernel, ep, tp, top), out_shape=[j...  109 us
    unnamed x5, local copies, waits for them, and re-layouts  5.21 us

profile of v3, /device:TPU:1, one launch (start us, length us, event | category | flops | bytes accessed | tf_op | source)
XLA Modules:
  0.0 118.3 jit_solution(1110523707174051068)
XLA Ops:
  0.6 0.7 compare_select_fusion.1
  1.3 0.2 fusion
  1.5 0.7 convert_add_fusion
  2.2 0.0 copy-start
  2.2 1.3 %compare_select_fusion = f32[1024]{0:T(1024)} fusion(f32[1024]{0:T(1024)} %param.28), kind=kLoop, calls=%fused_computation.5 | loop fusion | flops 7168 | bytes 8192 | tf_op jit(solution)/shard_map/jit(softplus)/select_n | solution.py:563
  3.5 0.8 copy.27.slots
  4.3 1.5 %copy.28.weights = f32[256,2]{1,0:T(8,128)} copy(f32[256,2]{0,1:T(2,128)} %param.34) | data formatting | bytes 4096 | tf_op args[13]
  5.8 0.0 copy-done
  5.8 108.7 %layer.1 = (bf16[64,4096]{1,0:T(8,128)(2,1)}, bf16[64,4096]{1,0:T(8,128)(2,1)}) custom-call(s32[256,2]{1,0:T(8,128)} %copy.27.slots, s32[2,256]{1,0:T(2,128)} %bitcast.13, f32[4,1024]{1,0:T(4,128)} %taps_ref.1, bf16[4,256,256]{2,1,0:T(8,128)(2,1)} %ig_ref.1, bf16[4,256,256]{2,1,0:T(8,128)(2,1)} %dg_ref.1, f32[1,1024]{1,0:T(1,128)} %bitcast.18, ...), custom_call_target="tpu_custom_call" | custom-call | tf_op jit(solution)/shard_map/layer/pallas_call | solution.py:482
  114.5 1.9 %copy.31 = bf16[64,4096]{1,0:T(8,128)(2,1)} copy(bf16[64,4096]{1,0:T(8,128)(2,1)} %get-tuple-element.4) | data formatting | bytes 1048576
  116.4 1.9 %copy.32 = bf16[64,4096]{1,0:T(8,128)(2,1)} copy(bf16[64,4096]{1,0:T(8,128)(2,1)} %get-tuple-element.5) | data formatting | bytes 1048576
  (2 shorter events, 0.1 us)
Async XLA Ops:
  2.2 3.6 %copy-start = (s32[256,2]{0,1:T(2,128)}, s32[256,2]{0,1:T(2,128)S(1)}, u32[]{:S(2)}) copy-start(s32[256,2]{0,1:T(2,128)S(1)} %convert_add_fusion) | copy-start | bytes 6148
